TPU v7x, 256 devices: a whole 4x4x8 slice. The times are simulated.
256 devices in a mesh: sp: 64 (over z, x, core), tp: 4 (over y).
Axes of the slice: x: 4, y: 4, z: 8, core: 2. Of those that a mesh axis runs over, the one named last changes fastest.
Arguments:
- moe_input: bfloat16 [8192, 2048], P('sp'), may hold values from -6 to 6
- out_cotangent: bfloat16 [8192, 2048], P('sp'), may hold values from -16 to 16
- routes: int32 [8192, 2], P('sp'), may hold values from 0 to 15, all different within a row; in each aligned block of 128 rows (0 to 127, 128 to 255, ...) at most 16 rows name the same one
- route_weight: float32 [8192, 2], P('sp'), may hold values from 0.2 to 1
- w_gate: bfloat16 [64, 2048, 896], P('sp', None, 'tp'), may hold values from -0.125 to 0.125
- w_up: bfloat16 [64, 2048, 896], P('sp', None, 'tp'), may hold values from -0.125 to 0.125
- w_down: bfloat16 [64, 896, 2048], P('sp', 'tp'), may hold values from -0.09375 to 0.09375
- out_proj: bfloat16 [2048, 1024], P(None, 'tp'), may hold values from -0.243067956 to 0.243067956
- conv_out: bfloat16 [8192, 1024], P('sp', 'tp'), may hold values from -17 to 17
- glu_value: bfloat16 [8192, 1024], P('sp', 'tp'), may hold values from -6 to 6
- glu_gate: bfloat16 [8192, 1024], P('sp', 'tp'), may hold values from -9 to 9
- taps: float32 [31, 1024], P(None, 'tp'), may hold values from -1 to 1
- norm_gain: float32 [1024], P('tp'), may hold values from 0.1 to 1.9
Outputs:
- grad_gate: bfloat16 [64, 2048, 896], P('sp', None, 'tp')
- grad_up: bfloat16 [64, 2048, 896], P('sp', None, 'tp')
- grad_down: bfloat16 [64, 896, 2048], P('sp', 'tp')
- grad_proj: float32 [2048, 1024], P('sp', 'tp')
- grad_glu_value: bfloat16 [8192, 1024], P('sp', 'tp')
- grad_glu_gate: bfloat16 [8192, 1024], P('sp', 'tp')
Inputs may be any that keep to these rules, and one draw needn't show every extreme that they name: `routes`: each token names two different experts. Within the 128 tokens of one index of sp no expert is named more than 16 times, a bound that some block reaches.
All inputs are finite; a program needn't handle non-finite values.
Results may differ from a plain program's by a relative error of at most 0.014.
Values may be sent and summed in bfloat16 or wider, within the bound.
No kernel may reach another device: no remote copies, remote signals or barrier semaphores. Data moves between devices by JAX's collectives and lax.ppermute only.
A program may use at most 128 MiB of HBM per device.

v0:
```python
import jax
import jax.numpy as jnp
from jax import lax
from jax.experimental import pallas as pl
from jax.experimental.pallas import tpu as pltpu
from jax.sharding import Mesh, PartitionSpec as P


DB = 1024
WIDTH = 31
EXPERTS = 16
CAP = 16
NZ, NX, NC, NY = 8, 4, 2, 4
ZX = NZ * NX
SP = ("z", "x", "c")
F32 = jnp.float32
BF16 = jnp.bfloat16


VMEM = pl.BlockSpec(memory_space=pltpu.VMEM)
HBM = pl.BlockSpec(memory_space=pl.ANY)
CONTRACT_FIRST = (((0,), (0,)), ((), ()))
CONTRACT_LAST = (((1,), (1,)), ((), ()))


def to_y(v, d):
    return lax.ppermute(v, "y", [(i, (i + d) % NY) for i in range(NY)])


def to_x(v):
    return lax.ppermute(v, "x", [(i, i ^ 1) for i in range(NX)])


def to_xy(v, d):
    pairs = [(x * NY + i, (x ^ 1) * NY + (i + d) % NY) for x in range(NX) for i in range(NY)]
    return lax.ppermute(v, ("x", "y"), pairs)


def to_c(v):
    return lax.ppermute(v, "c", [(0, 1), (1, 0)])


def swish_slope(pre, sig):
    return sig * (1.0 + pre * (1.0 - sig))


def own_col(dx, dy):
    block = lax.rem(lax.axis_index("y") + dy, NY)
    return 256 * (2 * block + lax.rem(lax.axis_index("x") + dx, 2))


def own_quarter():
    return pl.ds(pl.multiple_of(512 * lax.axis_index("y"), 512), 512)


def prep_body(routes, weights, all_rows, all_cots, send, places, own_cot, rows, cots, sems):
    copies = [
        pltpu.make_async_copy(src.at[:, own_quarter()], dst, sems.at[i])
        for i, (src, dst) in enumerate(((all_rows, rows), (all_cots, cots)))
    ]
    for copy in copies:
        copy.start()
    lane = lax.broadcasted_iota(jnp.int32, (EXPERTS, 128), 0)
    first = (lane == routes[0:1, :]).astype(F32)
    second = (lane == routes[1:2, :]).astype(F32)
    before = (
        lax.broadcasted_iota(jnp.int32, (128, 128), 0)
        < lax.broadcasted_iota(jnp.int32, (128, 128), 1)
    ).astype(BF16)
    earlier = jnp.dot((first + second).astype(BF16), before, preferred_element_type=F32)
    slot0 = jnp.sum(earlier * first, axis=0, keepdims=True).astype(jnp.int32)
    slot1 = jnp.sum(earlier * second, axis=0, keepdims=True).astype(jnp.int32)
    place = lax.broadcasted_iota(jnp.int32, (EXPERTS * CAP, 128), 0)
    hit0 = place == routes[0:1, :] * CAP + slot0
    hit1 = place == routes[1:2, :] * CAP + slot1
    scale = jnp.sum(
        jnp.where(hit0, weights[0:1, :], 0.0) + jnp.where(hit1, weights[1:2, :], 0.0),
        axis=1,
        keepdims=True,
    )
    pick = jnp.where(hit0 | hit1, 1.0, 0.0).astype(BF16)
    places[...] = pick
    for copy in copies:
        copy.wait()
    own_cot[...] = cots[...]
    sent_rows = jnp.dot(pick, rows[...], preferred_element_type=F32).astype(BF16)
    sent_cots = (scale * jnp.dot(pick, cots[...], preferred_element_type=F32)).astype(BF16)
    for half in range(2):
        cols = slice(256 * half, 256 * half + 256)
        send[:, half, 0] = sent_rows[:, cols].reshape(EXPERTS, CAP, 256)
        send[:, half, 1] = sent_cots[:, cols].reshape(EXPERTS, CAP, 256)


def prep(routes, weights, rows, cots):
    return pl.pallas_call(
        prep_body,
        out_shape=(
            jax.ShapeDtypeStruct((EXPERTS, 2, 2, CAP, 256), BF16),
            jax.ShapeDtypeStruct((EXPERTS * CAP, 128), BF16),
            jax.ShapeDtypeStruct((128, 512), BF16),
        ),
        in_specs=[VMEM, VMEM, HBM, HBM],
        out_specs=(VMEM,) * 3,
        scratch_shapes=[
            pltpu.VMEM((128, 512), BF16),
            pltpu.VMEM((128, 512), BF16),
            pltpu.SemaphoreType.DMA((2,)),
        ],
        name="prep",
    )(routes, weights, rows, cots)


BLOCKS = ((0, 0), (0, 3), (0, 1), (1, 0), (1, 3), (1, 1), (0, 2), (1, 2))
STAGES = ((0, 4), (4, 7), (7, 8))
HALF = ZX // 2
LAYOUTS = (
    ((0, 0, ZX), (1, 0, ZX), (2, 0, ZX), (3, 0, ZX)),
    ((0, 0, ZX), (1, 0, ZX), (2, 0, ZX)),
    ((0, 0, HALF), (0, HALF, HALF)),
)


def gather_first(v):
    return v, to_y(v, 1), to_y(v, -1), to_x(v)


def gather_second(first):
    _, behind, _, beside = first
    return to_x(behind), to_y(beside, -1), to_y(behind, 1)


def gather_third(second):
    return to_y(second[0][:HALF], 1), to_y(second[1][HALF:], -1)


def weights_in_order_body(*refs):
    for i in range(3):
        for stage, (lo, hi) in enumerate(STAGES):
            out = refs[6 + 3 * i + stage]
            for block in range(lo, hi):
                at = pl.ds(pl.multiple_of(own_col(*BLOCKS[block]), 256), 256)
                cols = slice(256 * (block - lo), 256 * (block - lo + 1))
                for side in range(2):
                    out[224 * side : 224 * side + 224, cols] = refs[2 * i + side][:, at]


def weights_in_order(flat):
    out = tuple(jax.ShapeDtypeStruct((448, 256 * (hi - lo)), BF16) for lo, hi in STAGES)
    res = pl.pallas_call(
        weights_in_order_body,
        out_shape=out * 3,
        in_specs=[VMEM] * 6,
        out_specs=(VMEM,) * 9,
        name="weights_in_order",
    )(*flat)
    return [(res[s], res[3 + s], res[6 + s]) for s in range(3)]


def put_pieces(pieces, layout, rows, cots):
    for piece, (block, first, count) in zip(pieces, layout):
        cols = slice(256 * block, 256 * block + 256)
        span = slice(first * CAP, (first + count) * CAP)
        rows[span, cols] = piece[:, 0].reshape(count * CAP, 256)
        cots[span, cols] = piece[:, 1].reshape(count * CAP, 256)


def stage_pass(stage, pieces, weights, before):
    layout = LAYOUTS[stage]
    n = len(layout)
    width = 256 * (STAGES[stage][1] - STAGES[stage][0])

    def body(*refs):
        given = refs[n + 3 : n + 3 + len(before)]
        rows, cots, *sums = refs[n + 3 + len(before) :]
        put_pieces(refs[:n], layout, rows, cots)
        for i, left in enumerate((rows, rows, cots)):
            part = lax.dot_general(
                left[...], refs[n + i][...], CONTRACT_LAST, preferred_element_type=F32
            )
            sums[i][...] = part + given[i][...] if before else part

    return pl.pallas_call(
        body,
        out_shape=(jax.ShapeDtypeStruct((ZX * CAP, width), BF16),) * 2
        + (jax.ShapeDtypeStruct((ZX * CAP, 448), F32),) * 3,
        in_specs=[VMEM] * (n + 3 + len(before)),
        out_specs=(VMEM,) * 5,
        input_output_aliases={n + 3 + i: 2 + i for i in range(len(before))},
    )(*pieces, *weights, *before)


def weights_of(block, gates):
    stage = next(s for s, (lo, hi) in enumerate(STAGES) if lo <= block < hi)
    at = 256 * (block - STAGES[stage][0])
    return gates[stage][:, at : at + 256]


def row_grads(d_gate, d_up, gate_w, up_w, blocks, grads):
    for block, grad in zip(blocks, grads):
        part = jnp.dot(
            d_gate[...], weights_of(block, gate_w), preferred_element_type=F32
        ) + jnp.dot(d_up[...], weights_of(block, up_w), preferred_element_type=F32)
        grad[...] = part.astype(BF16).reshape(ZX, CAP, 256)


FAR = (5, 4, 6, 7)
NEAR = (2, 1, 3, 0)


def last_body(*refs):
    pieces = refs[:2]
    gate_w, up_w, down_w = refs[2:5], refs[5:8], refs[8]
    before = refs[9:12]
    rows, cots, act, d_gate, d_up = refs[12:17]
    put_pieces(pieces, LAYOUTS[2], rows, cots)

    @pl.loop(0, 2)
    def _(m):
        span = pl.ds(pl.multiple_of(256 * m, 256), 256)
        gate, up, d_act = [
            before[i][span]
            + lax.dot_general(left[span], w[...], CONTRACT_LAST, preferred_element_type=F32)
            for i, (left, w) in enumerate(((rows, gate_w[2]), (rows, up_w[2]), (cots, down_w)))
        ]
        sig = jax.nn.sigmoid(gate)
        silu = gate * sig
        act[span] = (silu * up).astype(BF16)
        d_gate[span] = (d_act * up * swish_slope(gate, sig)).astype(BF16)
        d_up[span] = (d_act * silu).astype(BF16)

    row_grads(d_gate, d_up, gate_w, up_w, FAR, refs[17:21])


def last_pass(pieces, gate_w, up_w, down_w, before):
    n = ZX * CAP
    return pl.pallas_call(
        last_body,
        out_shape=(jax.ShapeDtypeStruct((n, 256), BF16),) * 2
        + (jax.ShapeDtypeStruct((n, 448), BF16),) * 3
        + (jax.ShapeDtypeStruct((ZX, CAP, 256), BF16),) * 4,
        in_specs=[VMEM] * 12,
        out_specs=(VMEM,) * 9,
        name="last_stage",
    )(*pieces, *gate_w, *up_w, down_w, *before)


def near_body(*refs):
    row_grads(refs[0], refs[1], refs[2:5], refs[5:8], NEAR, refs[8:12])


def near_pass(d_gate, d_up, gate_w, up_w):
    return pl.pallas_call(
        near_body,
        out_shape=(jax.ShapeDtypeStruct((ZX, CAP, 256), BF16),) * 4,
        in_specs=[VMEM] * 8,
        out_specs=(VMEM,) * 4,
        name="near_rows",
    )(d_gate, d_up, *gate_w, *up_w)


def weights_body(*refs):
    rows, cots = refs[0:3], refs[3:6]
    act, d_gate, d_up = refs[6:9]
    outs = refs[9:15]
    turned = refs[15]
    half = 224
    for i, (left, rights) in enumerate(((d_gate, rows), (d_up, rows), (act, cots))):
        turned[...] = left[...].T
        for stage, (lo, hi) in enumerate(STAGES):
            for block in range(lo, hi):
                at = slice(256 * (block - lo), 256 * (block - lo + 1))
                grad = jnp.dot(turned[...], rights[stage][:, at], preferred_element_type=F32)
                grad = grad.astype(BF16)
                to = pl.ds(pl.multiple_of(own_col(*BLOCKS[block]), 256), 256)
                outs[i][:, to] = grad[:half]
                outs[3 + i][:, to] = grad[half:]


def expert_weights_pass(rows, cots, act, d_gate, d_up):
    out = jax.ShapeDtypeStruct((act.shape[1] // 2, 2048), BF16)
    return pl.pallas_call(
        weights_body,
        out_shape=(out,) * 6,
        in_specs=[VMEM] * 9,
        out_specs=(VMEM,) * 6,
        scratch_shapes=[pltpu.VMEM((448, ZX * CAP), BF16)],
        name="expert_weights",
    )(*rows, *cots, act, d_gate, d_up)


def finish_body(*refs):
    for i in range(3):
        total = refs[i][...].astype(F32) + refs[3 + i][...].astype(F32)
        refs[6 + i][...] = total.astype(BF16)


def finish(own, others):
    out = jax.ShapeDtypeStruct(own[0].shape, BF16)
    return pl.pallas_call(
        finish_body,
        out_shape=(out,) * 3,
        in_specs=[VMEM] * 6,
        out_specs=(VMEM,) * 3,
        name="finish",
    )(*own, *others)


def combine_body(returned, places, cot, out):
    for half in range(2):
        cols = slice(256 * half, 256 * half + 256)
        slots = returned[:, half].reshape(EXPERTS * CAP, 256)
        moe = lax.dot_general(places[...], slots, CONTRACT_FIRST, preferred_element_type=F32)
        out[:, cols] = (cot[:, cols].astype(F32) + moe).astype(BF16)


def combine(returned, places, cot):
    return pl.pallas_call(
        combine_body,
        out_shape=jax.ShapeDtypeStruct(cot.shape, BF16),
        in_specs=[VMEM] * 3,
        out_specs=VMEM,
        name="combine",
    )(returned, places, cot)


def proj_body(own, one, two, three, mixed, resid, keep, send, table):
    y = lax.axis_index("y")
    for d, piece in enumerate((own, one, two, three)):
        block = lax.rem(y + (NY - d), NY)
        resid[:, pl.ds(pl.multiple_of(block * 512, 512), 512)] = piece[...]
        part = lax.dot_general(piece[...], mixed[...], CONTRACT_FIRST, preferred_element_type=F32)
        table[pl.ds(block * 8, 8)] = part.astype(BF16).reshape(8, 2, 32, 256)
    core = lax.axis_index("c")
    keep[...] = table[:, core]
    send[...] = table[:, 1 - core]


def proj(pieces, mixed):
    return pl.pallas_call(
        proj_body,
        out_shape=(
            jax.ShapeDtypeStruct((128, 2048), BF16),
            jax.ShapeDtypeStruct((ZX, 32, 256), BF16),
            jax.ShapeDtypeStruct((ZX, 32, 256), BF16),
        ),
        in_specs=[VMEM] * 5,
        out_specs=(VMEM,) * 3,
        scratch_shapes=[pltpu.VMEM((ZX, 2, 32, 256), BF16)],
        name="proj",
    )(*pieces, mixed)


def channels_body(resid, out_proj, normed, gain, d_norm, sums):
    d_mixed = jnp.dot(resid[...], out_proj[...], preferred_element_type=F32)
    zpre = normed[...] * gain[...]
    grad = d_mixed * swish_slope(zpre, jax.nn.sigmoid(zpre)) * gain[...]
    d_norm[...] = grad
    first = jnp.sum(grad, axis=1, keepdims=True)
    second = jnp.sum(grad * normed[...], axis=1, keepdims=True)
    lane = lax.broadcasted_iota(jnp.int32, (128, 128), 1)
    table = jnp.where(lane == 0, first, jnp.where(lane == 1, second, 0.0))
    sums[...] = table.T[0:8]


def channels(resid, out_proj, normed, gain):
    return pl.pallas_call(
        channels_body,
        out_shape=(
            jax.ShapeDtypeStruct(normed.shape, F32),
            jax.ShapeDtypeStruct((8, 128), F32),
        ),
        in_specs=[VMEM] * 4,
        out_specs=(VMEM,) * 2,
        name="channels",
    )(resid, out_proj, normed, gain)


def sum_over_y(v):
    return v + to_y(v, 1) + to_y(v, -1) + to_y(v, 2)


def step(
    moe_input,
    out_cotangent,
    routes,
    route_weight,
    w_gate,
    w_up,
    w_down,
    out_proj,
    conv_out,
    glu_value,
    glu_gate,
    taps,
    norm_gain,
):
    send, places, own_cot = prep(routes.T, route_weight.T, moe_input, out_cotangent)
    shard = lax.all_to_all(send.reshape(ZX, 2, CAP, 256), ("z", "x"), 0, 0, tiled=True)
    own_w = (w_gate[0].T, w_up[0].T, w_down[0])
    ordered = weights_in_order([v for w in own_w for v in (w, to_c(w))])
    shard, ordered = lax.optimization_barrier((shard, ordered))
    gate_w, up_w, down_w = zip(*ordered)
    first = gather_first(shard)
    second = gather_second(first)
    rows0, cots0, *sums = stage_pass(0, first, ordered[0], ())
    third = gather_third(second)
    rows1, cots1, *sums = stage_pass(1, second, ordered[1], sums)
    rows2, cots2, act, d_gate, d_up, *far = last_pass(third, gate_w, up_w, down_w[2], sums)
    far = (to_xy(far[0], 1), to_xy(far[1], -1), to_y(far[2], 2), to_xy(far[3], 2))
    near = near_pass(d_gate, d_up, gate_w, up_w)
    near = (near[3], to_y(near[0], 1), to_y(near[1], -1), to_x(near[2]))
    weight_grads = expert_weights_pass(
        (rows0, rows1, rows2), (cots0, cots1, cots2), act, d_gate, d_up
    )
    total = near[0].astype(F32)
    for part in (*far, *near[1:]):
        total = total + part.astype(F32)
    total = total.astype(BF16)
    returned = lax.all_to_all(total, ("z", "x"), 0, 0, tiled=True)
    resid_part = combine(returned.reshape(EXPERTS, 2, CAP, 256), places, own_cot)
    resid_pieces = (
        resid_part,
        to_y(resid_part, 1),
        to_y(resid_part, 2),
        to_y(resid_part, 3),
    )
    others = [to_c(other) for other in weight_grads[3:]]
    grad_gate, grad_up, grad_down = finish(weight_grads[:3], others)

    conv_vals = conv_out.astype(F32)
    sums = sum_over_y(
        jnp.stack([jnp.sum(conv_vals, axis=1), jnp.sum(conv_vals * conv_vals, axis=1)])
    )
    mean = sums[0][:, None] / DB
    rstd = lax.rsqrt(sums[1][:, None] / DB - mean * mean + 1e-05)
    normed = (conv_vals - mean) * rstd
    zpre = normed * norm_gain[None, :]
    zsig = jax.nn.sigmoid(zpre)
    mixed = (zpre * zsig).astype(BF16)

    resid_grad, keep, give = proj(resid_pieces, mixed)
    by_owner = (keep.astype(F32) + to_c(give).astype(F32)).astype(BF16)
    resid_grad, by_owner = lax.optimization_barrier((resid_grad, by_owner))
    owned = lax.all_to_all(by_owner, ("z", "x"), 0, 0, tiled=True)
    grad_proj = jnp.sum(owned.astype(F32), axis=0)

    d_norm, sums = channels(resid_grad, out_proj, normed, norm_gain[None, :])
    sums = sum_over_y(sums)
    conv_grad = (
        rstd * (d_norm - sums[0][:, None] / DB - normed * sums[1][:, None] / DB)
    ).astype(BF16)
    n_sp = NZ * NX * NC
    later_rows = lax.ppermute(conv_grad[: WIDTH - 1], SP, [(i, i - 1) for i in range(1, n_sp)])
    extended = jnp.concatenate([conv_grad, later_rows], axis=0).astype(F32)
    unit_grad = lax.conv_general_dilated(
        extended[None],
        taps[:, None, :],
        (1,),
        "VALID",
        dimension_numbers=("NWC", "WIO", "NWC"),
        feature_group_count=taps.shape[1],
        precision=lax.Precision.HIGHEST,
    )[0]
    gate_sig_in = jax.nn.sigmoid(glu_gate.astype(F32))
    grad_glu_value = (unit_grad * gate_sig_in).astype(BF16)
    grad_glu_gate = (
        unit_grad * glu_value.astype(F32) * gate_sig_in * (1.0 - gate_sig_in)
    ).astype(BF16)
    return (
        grad_gate.T[None],
        grad_up.T[None],
        grad_down[None],
        grad_proj,
        grad_glu_value,
        grad_glu_gate,
    )


def solution(mesh):
    wide = Mesh(mesh.devices.reshape(NZ, NX, NC, NY), ("z", "x", "c", "y"))
    in_specs = (
        P(SP, None),
        P(SP, None),
        P(SP, None),
        P(SP, None),
        P(SP, None, "y"),
        P(SP, None, "y"),
        P(SP, "y", None),
        P(None, "y"),
        P(SP, "y"),
        P(SP, "y"),
        P(SP, "y"),
        P(None, "y"),
        P("y"),
    )
    out_specs = (
        P(SP, None, "y"),
        P(SP, None, "y"),
        P(SP, "y", None),
        P(SP, "y"),
        P(SP, "y"),
        P(SP, "y"),
    )
    return jax.shard_map(step, mesh=wide, in_specs=in_specs, out_specs=out_specs, check_vma=False)
```

profile of v0, /device:TPU:1, one launch (start us, length us, event | category | flops | bytes accessed | tf_op | source)
XLA Modules:
  0.0 198.5 jit_solution(9426475026680815825)
XLA Ops:
  0.7 3.0 %prep.1 = (bf16[16,2,2,16,256]{4,3,2,1,0:T(8,128)(2,1)}, bf16[256,128]{1,0:T(8,128)(2,1)}, bf16[128,512]{1,0:T(8,128)(2,1)}) custom-call(s32[2,128]{1,0:T(2,128)} %bitcast.63, f32[2,128]{1,0:T(2,128)} %bitcast.64, bf16[128,2048]{1,0:T(8,128)(2,1)} %all_rows.1, bf16[128,2048]{1,0:T(8,128)(2,1)} %all_cots.1), custom_call_target="tpu_custom_call" | custom-call | tf_op jit(solution)/shard_map/prep/pallas_call | solution.py:95
  3.6 11.9 %all-to-all-start = ((bf16[32,2,16,256]{3,2,1,0:T(8,128)(2,1)}), bf16[32,2,16,256]{3,2,1,0:T(8,128)(2,1)S(1)}, u32[]{:S(2)}, u32[]{:S(2)}) async-start(bf16[32,2,16,256]{3,2,1,0:T(8,128)(2,1)} %bitcast.57), calls=%async_computation | async-start | bytes 1048576 | tf_op jit(solution)/shard_map/all_to_all | solution.py:398
  15.5 1.0 collective-permute-start
  17.1 1.6 collective-permute-done.refs_1_
  18.7 1.3 collective-permute-done.1.refs_3_
  21.4 5.8 %weights_in_order.1 = (bf16[448,1024]{1,0:T(8,128)(2,1)}, bf16[448,768]{1,0:T(8,128)(2,1)}, bf16[448,256]{1,0:T(8,128)(2,1)}, bf16[448,1024]{1,0:T(8,128)(2,1)},...) custom-call(bf16[224,2048]{1,0:T(8,128)(2,1)} %bitcast.51, ...), custom_call_target="tpu_custom_call" | custom-call | tf_op jit(solution)/shard_map/weights_in_order/pallas_call | solution.py:149
  27.2 4.6 %all-to-all-done.refs_0_ = bf16[32,2,16,256]{3,2,1,0:T(8,128)(2,1)S(1)} async-done(((bf16[32,2,16,256]{3,2,1,0:T(8,128)(2,1)}), bf16[32,2,16,256]{3,2,1,0:T(8,128)(2,1)S(1)}, u32[]{:S(2)}, u32[]{:S(2)}) %all-to-all-start) | async-done | bytes 524320 | tf_op jit(solution)/shard_map/all_to_all | solution.py:398
  31.8 1.3 collective-permute-start.3
  33.1 1.0 collective-permute-start.5
  34.1 10.1 %collective-permute-done.3.refs_1_ = bf16[32,2,16,256]{3,2,1,0:T(8,128)(2,1)S(1)} collective-permute-done((bf16[32,2,16,256]{3,2,1,0:T(8,128)(2,1)S(1)}, bf16[32,2,16,256]{3,2,1,0:T(8,128)(2,1)S(1)}, u32[]{:S(2)}, u32[]{:S(2)}) %collective-permute-start.3) | collective-permute-done | bytes 524320 | tf_op jit(solution)/shard_map/ppermute | solution.py:27
  44.2 1.5 collective-permute-start.6
  45.7 1.4 collective-permute-start.7
  47.5 1.0 collective-permute-start.8
  48.5 6.2 %collective-permute-done.6.refs_0_ = bf16[32,2,16,256]{3,2,1,0:T(8,128)(2,1)S(1)} collective-permute-done((bf16[32,2,16,256]{3,2,1,0:T(8,128)(2,1)S(1)}, bf16[32,2,16,256]{3,2,1,0:T(8,128)(2,1)S(1)}, u32[]{:S(2)}, u32[]{:S(2)}) %collective-permute-start.6) | collective-permute-done | bytes 524320 | tf_op jit(solution)/shard_map/ppermute | solution.py:31
  54.8 2.6 %collective-permute-start.9 = (bf16[16,2,16,256]{3,2,1,0:T(8,128)(2,1)S(1)}, bf16[16,2,16,256]{3,2,1,0:T(8,128)(2,1)S(1)}, u32[]{:S(2)}, u32[]{:S(2)}) collective-permute-start(bf16[16,2,16,256]{3,2,1,0:T(8,128)(2,1)S(1)} %slice.28), channel_id=1, source_target_pairs={{0,1},{1,2},{2,3},{3,0},{4,5},{5,6},{6,7},{7,4},{8,9},{9,10},{10,1... | collective-permute-start | bytes 786440 | tf_op jit(solution)/shard_map/ppermute | solution.py:27
  57.4 1.5 collective-permute-start.10
  59.0 8.5 %collective-permute-done.4.refs_2_ = bf16[32,2,16,256]{3,2,1,0:T(8,128)(2,1)} collective-permute-done((bf16[32,2,16,256]{3,2,1,0:T(8,128)(2,1)S(1)}, bf16[32,2,16,256]{3,2,1,0:T(8,128)(2,1)}, u32[]{:S(2)}, u32[]{:S(2)}) %collective-permute-start.4) | collective-permute-done | bytes 524320 | tf_op jit(solution)/shard_map/ppermute | solution.py:27
  67.4 5.7 %shard_map.172 = (bf16[512,1024]{1,0:T(8,128)(2,1)}, bf16[512,1024]{1,0:T(8,128)(2,1)}, f32[512,448]{1,0:T(8,128)}, f32[512,448]{1,0:T(8,128)}, f32[512,448]{1,0:T(8,128)}) custom-call(bf16[32,2,16,256]{3,2,1,0:T(8,128)(2,1)} %copy-done.1, bf16[32,2,16,256]{3,2,1,0:T(8,128)(2,1)} %copy-done.13, bf16[32,2,16,256]{3,2,1,0:T(8,128)(2,1)} %collective-permute-done.4.refs_2_, ...), custom_call_target="tpu_custom_call" | custom-call | tf_op jit(solution)/shard_map/pallas_call | solution.py:182
  73.9 6.1 %shard_map.173 = (bf16[512,768]{1,0:T(8,128)(2,1)}, bf16[512,768]{1,0:T(8,128)(2,1)}, f32[512,448]{1,0:T(8,128)}, f32[512,448]{1,0:T(8,128)}, f32[512,448]{1,0:T(8,128)}) custom-call(bf16[32,2,16,256]{3,2,1,0:T(8,128)(2,1)} %copy-done.2, bf16[32,2,16,256]{3,2,1,0:T(8,128)(2,1)} %copy-done.3, ...), custom_call_target="tpu_custom_call", output_to_operand_aliasing={{2}: (6, {}), {3}: (7, {}), {4}: (8, {})} | custom-call | tf_op jit(solution)/shard_map/pallas_call | solution.py:182
  80.7 6.3 %last_stage.1 = (bf16[512,256]{1,0:T(8,128)(2,1)}, bf16[512,256]{1,0:T(8,128)(2,1)}, bf16[512,448]{1,0:T(8,128)(2,1)}, bf16[512,448]{1,0:T(8,128)(2,1)}, bf16[51...) custom-call(bf16[16,2,16,256]{3,2,1,0:T(8,128)(2,1)} %copy-done.17, ...), custom_call_target="tpu_custom_call" | custom-call | tf_op jit(solution)/shard_map/last_stage/pallas_call | solution.py:236
  87.1 4.4 %near_rows.1 = (bf16[32,16,256]{2,1,0:T(8,128)(2,1)}, bf16[32,16,256]{2,1,0:T(8,128)(2,1)}, bf16[32,16,256]{2,1,0:T(8,128)(2,1)}, bf16[32,16,256]{2,1,0:T(8,128)(2,1)}) custom-call(bf16[512,448]{1,0:T(8,128)(2,1)} %get-tuple-element.100.refs_7_.refs_0_, bf16[512,448]{1,0:T(8,128)(2,1)} %get-tuple-element.101.refs_8_.refs_1_, ...), custom_call_target="tpu_custom_call" | custom-call | tf_op jit(solution)/shard_map/near_rows/pallas_call | solution.py:252
  91.5 2.7 %collective-permute-start.19 = (bf16[32,16,256]{2,1,0:T(8,128)(2,1)}, bf16[32,16,256]{2,1,0:T(8,128)(2,1)S(1)}, u32[]{:S(2)}, u32[]{:S(2)}) collective-permute-start(bf16[32,16,256]{2,1,0:T(8,128)(2,1)} %get-tuple-element.117), channel_id=1, source_target_pairs={{0,3},{1,0},{2,1},{3,2},{4,7},{5,4},{6,5},{7,6},{8,11},{9,8},{10,9... | collective-permute-start | bytes 786440 | tf_op jit(solution)/shard_map/ppermute | solution.py:27
  94.2 3.6 %collective-permute-start.15 = (bf16[32,16,256]{2,1,0:T(8,128)(2,1)S(1)}, bf16[32,16,256]{2,1,0:T(8,128)(2,1)S(1)}, u32[]{:S(2)}, u32[]{:S(2)}) collective-permute-start(bf16[32,16,256]{2,1,0:T(8,128)(2,1)S(1)} %copy-done.27), channel_id=1, source_target_pairs={{0,11},{1,8},{2,9},{3,10},{8,3},{9,0},{10,1},{11,2},{16,27},{17,24... | collective-permute-start | bytes 786440 | tf_op jit(solution)/shard_map/ppermute | solution.py:36
  98.9 3.0 %collective-permute-start.17 = (bf16[32,16,256]{2,1,0:T(8,128)(2,1)S(1)}, bf16[32,16,256]{2,1,0:T(8,128)(2,1)S(1)}, u32[]{:S(2)}, u32[]{:S(2)}) collective-permute-start(bf16[32,16,256]{2,1,0:T(8,128)(2,1)S(1)} %copy-done.25), channel_id=1, source_target_pairs={{0,10},{1,11},{2,8},{3,9},{8,2},{9,3},{10,0},{11,1},{16,26},{17,27... | collective-permute-start | bytes 786440 | tf_op jit(solution)/shard_map/ppermute | solution.py:36
  102.2 1.7 collective-permute-done.14
  103.9 1.0 collective-permute-start.25
  104.9 3.2 %collective-permute-start.26 = (f32[2,128]{1,0:T(2,128)S(1)}, f32[2,128]{1,0:T(2,128)S(1)}, u32[]{:S(2)}, u32[]{:S(2)}) collective-permute-start(f32[2,128]{1,0:T(2,128)S(1)} %pad_maximum_fusion), channel_id=1, source_target_pairs={{0,2},{1,3},{2,0},{3,1},{4,6},{5,7},{6,4},{7,5},{8,10},{9,11},{10,... | collective-permute-start | bytes 3080 | tf_op jit(solution)/shard_map/ppermute | solution.py:27
  109.1 5.0 %collective-permute-done.17 = bf16[32,16,256]{2,1,0:T(8,128)(2,1)S(1)} collective-permute-done((bf16[32,16,256]{2,1,0:T(8,128)(2,1)S(1)}, bf16[32,16,256]{2,1,0:T(8,128)(2,1)S(1)}, u32[]{:S(2)}, u32[]{:S(2)}) %collective-permute-start.17) | collective-permute-done | bytes 262176 | tf_op jit(solution)/shard_map/ppermute | solution.py:36
  114.1 1.9 add_convert_fusion.1
  116.0 7.8 %all-to-all-start.1 = ((bf16[32,16,256]{2,1,0:T(8,128)(2,1)}), bf16[32,16,256]{2,1,0:T(8,128)(2,1)S(1)}, u32[]{:S(2)}, u32[]{:S(2)}) async-start(bf16[32,16,256]{2,1,0:T(8,128)(2,1)} %add_convert_fusion.1), calls=%async_computation.1 | async-start | bytes 524288 | tf_op jit(solution)/shard_map/all_to_all | solution.py:419
  123.9 10.3 %all-to-all-done.1 = bf16[32,16,256]{2,1,0:T(8,128)(2,1)S(1)} async-done(((bf16[32,16,256]{2,1,0:T(8,128)(2,1)}), bf16[32,16,256]{2,1,0:T(8,128)(2,1)S(1)}, u32[]{:S(2)}, u32[]{:S(2)}) %all-to-all-start.1) | async-done | bytes 262176 | tf_op jit(solution)/shard_map/all_to_all | solution.py:419
  134.9 1.9 combine.1.own
  136.8 1.4 collective-permute-start.21
  138.7 2.1 %collective-permute-start.23 = (bf16[128,512]{1,0:T(8,128)(2,1)}, bf16[128,512]{1,0:T(8,128)(2,1)S(1)}, u32[]{:S(2)}, u32[]{:S(2)}) collective-permute-start(bf16[128,512]{1,0:T(8,128)(2,1)} %combine.1.own), channel_id=1, source_target_pairs={{0,3},{1,0},{2,1},{3,2},{4,7},{5,4},{6,5},{7,6},{8,11},{9,8},{10,9... | collective-permute-start | bytes 393224 | tf_op jit(solution)/shard_map/ppermute | solution.py:27
  142.4 1.7 collective-permute-done.22.two
  145.0 2.9 %proj.1 = (bf16[128,2048]{1,0:T(8,128)(2,1)}, bf16[32,32,256]{2,1,0:T(8,128)(2,1)}, bf16[32,32,256]{2,1,0:T(8,128)(2,1)}) custom-call(bf16[128,512]{1,0:T(8,128)(2,1)} %combine.1.own, bf16[128,512]{1,0:T(8,128)(2,1)} %copy-done.18, bf16[128,512]{1,0:T(8,128)(2,1)} %copy-done.19, bf16[128,512]{1,0:T(8,128)(2,1)} %copy-done.20, ...), custom_call_target="tpu_custom_call" | custom-call | tf_op jit(solution)/shard_map/proj/pallas_call | solution.py:339
  147.9 14.9 %collective-permute-start.27 = (bf16[32,32,256]{2,1,0:T(8,128)(2,1)}, bf16[32,32,256]{2,1,0:T(8,128)(2,1)}, u32[]{:S(2)}, u32[]{:S(2)}) collective-permute-start(bf16[32,32,256]{2,1,0:T(8,128)(2,1)} %get-tuple-element.123), channel_id=1, source_target_pairs={{0,4},{4,0},{1,5},{5,1},{2,6},{6,2},{3,7},{7,3},{8,12},{12,8},{9,1... | collective-permute-start | bytes 1572872 | tf_op jit(solution)/shard_map/ppermute | solution.py:40
  162.8 7.1 %expert_weights.1 = (bf16[224,2048]{1,0:T(8,128)(2,1)}, bf16[224,2048]{1,0:T(8,128)(2,1)}, bf16[224,2048]{1,0:T(8,128)(2,1)}, bf16[224,2048]{1,0:T(8,128)(2,1)},...) custom-call(bf16[512,1024]{1,0:T(8,128)(2,1)} %get-tuple-element.81.refs_0_, ...), custom_call_target="tpu_custom_call" | custom-call | tf_op jit(solution)/shard_map/expert_weights/pallas_call | solution.py:281
  170.5 2.0 %add_convert_fusion = bf16[32,32,256]{2,1,0:T(8,128)(2,1)} fusion(bf16[32,32,256]{2,1,0:T(8,128)(2,1)} %collective-permute-done.27, bf16[32,32,256]{2,1,0:T(8,128)(2,1)S(1)} %copy-done.15), kind=kLoop, calls=%fused_computation.1 | loop fusion | flops 1048576 | bytes 1572864 | tf_op jit(solution)/shard_map/convert_element_type | solution.py:442
  172.5 2.4 %channels.1 = (f32[128,256]{1,0:T(8,128)}, f32[8,128]{1,0:T(8,128)}) custom-call(bf16[128,2048]{1,0:T(8,128)(2,1)} %get-tuple-element.125.resid, bf16[2048,256]{1,0:T(8,128)(2,1)} %out_proj.1, f32[128,256]{1,0:T(8,128)} %get-tuple-element.132.normed, f32[1,256]{1,0:T(1,128)} %bitcast.62), custom_call_target="tpu_custom_call" | custom-call | tf_op jit(solution)/shard_map/channels/pallas_call | solution.py:366
  174.9 2.7 %collective-permute-start.29 = (f32[8,128]{1,0:T(8,128)}, f32[8,128]{1,0:T(8,128)S(1)}, u32[]{:S(2)}, u32[]{:S(2)}) collective-permute-start(f32[8,128]{1,0:T(8,128)} %get-tuple-element.127), channel_id=1, source_target_pairs={{0,3},{1,0},{2,1},{3,2},{4,7},{5,4},{6,5},{7,6},{8,11},{9,8},{10,9... | collective-permute-start | bytes 12296 | tf_op jit(solution)/shard_map/ppermute | solution.py:27
  177.6 1.2 collective-permute-done.28
  178.8 3.9 %all-to-all-start.2 = ((bf16[32,32,256]{2,1,0:T(8,128)(2,1)}), bf16[32,32,256]{2,1,0:T(8,128)(2,1)S(1)}, u32[]{:S(2)}, u32[]{:S(2)}) async-start(bf16[32,32,256]{2,1,0:T(8,128)(2,1)} %add_convert_fusion), calls=%async_computation.2 | async-start | bytes 1048576 | tf_op jit(solution)/shard_map/all_to_all | solution.py:444
  183.0 1.0 multiply_convert_fusion
  184.0 4.7 %collective-permute-start.31 = (bf16[30,256]{1,0:T(8,128)(2,1)S(1)}, bf16[30,256]{1,0:T(8,128)(2,1)S(1)}, u32[]{:S(2)}, u32[]{:S(2)}) collective-permute-start(bf16[30,256]{1,0:T(8,128)(2,1)S(1)} %slice.30), channel_id=1, source_target_pairs={{4,0},{8,4},{12,8},{16,12},{20,16},{24,20},{28,24},{32,28},{36,32}... | collective-permute-start | bytes 46088 | tf_op jit(solution)/shard_map/ppermute | solution.py:453
  188.8 0.9 copy-done.7
  190.3 4.3 %finish.1 = (bf16[224,2048]{1,0:T(8,128)(2,1)}, bf16[224,2048]{1,0:T(8,128)(2,1)}, bf16[224,2048]{1,0:T(8,128)(2,1)}) custom-call(bf16[224,2048]{1,0:T(8,128)(2,1)} %get-tuple-element.102.refs_0_, bf16[224,2048]{1,0:T(8,128)(2,1)} %get-tuple-element.103.refs_1_, bf16[224,2048]{1,0:T(8,128)(2,1)} %get-tuple-element.104.refs_2_, bf16[224,2048]{1,0:T(8,128)(2,1)} %copy-done.7, ...), custom_call_target="tpu_custom_call" | custom-call | tf_op jit(solution)/shard_map/finish/pallas_call | solution.py:299
  196.2 1.6 all-to-all-done.2
  (109 shorter events, 13.6 us)
Async XLA Ops:
  0.6 193.9 %copy-start = (f32[31,256]{1,0:T(8,128)S(1)}, f32[31,256]{1,0:T(8,128)}, u32[]{:S(2)}) copy-start(f32[31,256]{1,0:T(8,128)} %param.24) | copy-start | bytes 95236
  0.6 14.9 %copy-start.5 = (bf16[1,2048,224]{1,2,0:T(8,128)(2,1)S(1)}, bf16[1,2048,224]{1,2,0:T(8,128)(2,1)}, u32[]{:S(2)}) copy-start(bf16[1,2048,224]{1,2,0:T(8,128)(2,1)} %param.17) | copy-start | bytes 2752516
  0.7 15.9 %copy-start.6 = (bf16[1,2048,224]{1,2,0:T(8,128)(2,1)S(1)}, bf16[1,2048,224]{1,2,0:T(8,128)(2,1)}, u32[]{:S(2)}) copy-start(bf16[1,2048,224]{1,2,0:T(8,128)(2,1)} %param.18) | copy-start | bytes 2752516
  3.6 28.2 %all-to-all-start = ((bf16[32,2,16,256]{3,2,1,0:T(8,128)(2,1)}), bf16[32,2,16,256]{3,2,1,0:T(8,128)(2,1)S(1)}, u32[]{:S(2)}, u32[]{:S(2)}) async-start(bf16[32,2,16,256]{3,2,1,0:T(8,128)(2,1)} %bitcast.57), calls=%async_computation | async-start | bytes 1048576 | tf_op jit(solution)/shard_map/all_to_all | solution.py:398
  15.5 3.1 %collective-permute-start = (bf16[224,2048]{1,0:T(8,128)(2,1)S(1)}, bf16[224,2048]{1,0:T(8,128)(2,1)S(1)}, u32[]{:S(2)}, u32[]{:S(2)}) collective-permute-start(bf16[224,2048]{1,0:T(8,128)(2,1)S(1)} %bitcast.52), channel_id=1, source_target_pairs={{0,4},{4,0},{1,5},{5,1},{2,6},{6,2},{3,7},{7,3},{8,12},{12,8},{9,1... | collective-permute-start | bytes 2752520 | tf_op jit(solution)/shard_map/ppermute | solution.py:40
  16.6 3.4 %collective-permute-start.1 = (bf16[224,2048]{1,0:T(8,128)(2,1)S(1)}, bf16[224,2048]{1,0:T(8,128)(2,1)S(1)}, u32[]{:S(2)}, u32[]{:S(2)}) collective-permute-start(bf16[224,2048]{1,0:T(8,128)(2,1)S(1)} %bitcast.54), channel_id=1, source_target_pairs={{0,4},{4,0},{1,5},{5,1},{2,6},{6,2},{3,7},{7,3},{8,12},{12,8},{9,1... | collective-permute-start | bytes 2752520 | tf_op jit(solution)/shard_map/ppermute | solution.py:40
  16.7 4.7 %collective-permute-start.2 = (bf16[224,2048]{1,0:T(8,128)(2,1)}, bf16[224,2048]{1,0:T(8,128)(2,1)}, u32[]{:S(2)}, u32[]{:S(2)}) collective-permute-start(bf16[224,2048]{1,0:T(8,128)(2,1)} %bitcast.55), channel_id=1, source_target_pairs={{0,4},{4,0},{1,5},{5,1},{2,6},{6,2},{3,7},{7,3},{8,12},{12,8},{9,1... | collective-permute-start | bytes 2752520 | tf_op jit(solution)/shard_map/ppermute | solution.py:40
  31.8 25.6 %copy-start.1 = (bf16[32,2,16,256]{3,2,1,0:T(8,128)(2,1)}, bf16[32,2,16,256]{3,2,1,0:T(8,128)(2,1)S(1)}, u32[]{:S(2)}) copy-start(bf16[32,2,16,256]{3,2,1,0:T(8,128)(2,1)S(1)} %all-to-all-done.refs_0_) | copy-start | bytes 1572868
  31.8 12.4 %collective-permute-start.3 = (bf16[32,2,16,256]{3,2,1,0:T(8,128)(2,1)S(1)}, bf16[32,2,16,256]{3,2,1,0:T(8,128)(2,1)S(1)}, u32[]{:S(2)}, u32[]{:S(2)}) collective-permute-start(bf16[32,2,16,256]{3,2,1,0:T(8,128)(2,1)S(1)} %all-to-all-done.refs_0_), channel_id=1, source_target_pairs={{0,1},{1,2},{2,3},{3,0},{4,5},{5,6},{6,7},{7,4},{8,9},{9,10},{10,1... | collective-permute-start | bytes 1572872 | tf_op jit(solution)/shard_map/ppermute | solution.py:27
  33.1 12.6 %collective-permute-start.5 = (bf16[32,2,16,256]{3,2,1,0:T(8,128)(2,1)S(1)}, bf16[32,2,16,256]{3,2,1,0:T(8,128)(2,1)S(1)}, u32[]{:S(2)}, u32[]{:S(2)}) collective-permute-start(bf16[32,2,16,256]{3,2,1,0:T(8,128)(2,1)S(1)} %all-to-all-done.refs_0_), channel_id=1, source_target_pairs={{0,8},{8,0},{16,24},{24,16},{1,9},{9,1},{17,25},{25,17},{2,10},{10... | collective-permute-start | bytes 1572872 | tf_op jit(solution)/shard_map/ppermute | solution.py:31
  44.2 23.3 %copy-start.13 = (bf16[32,2,16,256]{3,2,1,0:T(8,128)(2,1)}, bf16[32,2,16,256]{3,2,1,0:T(8,128)(2,1)S(1)}, u32[]{:S(2)}) copy-start(bf16[32,2,16,256]{3,2,1,0:T(8,128)(2,1)S(1)} %collective-permute-done.3.refs_1_) | copy-start | bytes 1572868
  44.2 10.5 %collective-permute-start.6 = (bf16[32,2,16,256]{3,2,1,0:T(8,128)(2,1)S(1)}, bf16[32,2,16,256]{3,2,1,0:T(8,128)(2,1)S(1)}, u32[]{:S(2)}, u32[]{:S(2)}) collective-permute-start(bf16[32,2,16,256]{3,2,1,0:T(8,128)(2,1)S(1)} %collective-permute-done.3.refs_1_), channel_id=1, source_target_pairs={{0,8},{8,0},{16,24},{24,16},{1,9},{9,1},{17,25},{25,17},{2,10},{10... | collective-permute-start | bytes 1572872 | tf_op jit(solution)/shard_map/ppermute | solution.py:31
  45.7 21.8 %copy-start.14 = (bf16[32,2,16,256]{3,2,1,0:T(8,128)(2,1)}, bf16[32,2,16,256]{3,2,1,0:T(8,128)(2,1)S(1)}, u32[]{:S(2)}) copy-start(bf16[32,2,16,256]{3,2,1,0:T(8,128)(2,1)S(1)} %collective-permute-done.5.refs_3_) | copy-start | bytes 1572868
  45.7 11.7 %collective-permute-start.7 = (bf16[32,2,16,256]{3,2,1,0:T(8,128)(2,1)S(1)}, bf16[32,2,16,256]{3,2,1,0:T(8,128)(2,1)S(1)}, u32[]{:S(2)}, u32[]{:S(2)}) collective-permute-start(bf16[32,2,16,256]{3,2,1,0:T(8,128)(2,1)S(1)} %collective-permute-done.5.refs_3_), channel_id=1, source_target_pairs={{0,3},{1,0},{2,1},{3,2},{4,7},{5,4},{6,5},{7,6},{8,11},{9,8},{10,9... | collective-permute-start | bytes 1572872 | tf_op jit(solution)/shard_map/ppermute | solution.py:27
  47.1 20.4 %collective-permute-start.4 = (bf16[32,2,16,256]{3,2,1,0:T(8,128)(2,1)S(1)}, bf16[32,2,16,256]{3,2,1,0:T(8,128)(2,1)}, u32[]{:S(2)}, u32[]{:S(2)}) collective-permute-start(bf16[32,2,16,256]{3,2,1,0:T(8,128)(2,1)S(1)} %all-to-all-done.refs_0_), channel_id=1, source_target_pairs={{0,3},{1,0},{2,1},{3,2},{4,7},{5,4},{6,5},{7,6},{8,11},{9,8},{10,9... | collective-permute-start | bytes 1572872 | tf_op jit(solution)/shard_map/ppermute | solution.py:27
  47.5 25.6 %collective-permute-start.8 = (bf16[32,2,16,256]{3,2,1,0:T(8,128)(2,1)S(1)}, bf16[32,2,16,256]{3,2,1,0:T(8,128)(2,1)S(1)}, u32[]{:S(2)}, u32[]{:S(2)}) collective-permute-start(bf16[32,2,16,256]{3,2,1,0:T(8,128)(2,1)S(1)} %collective-permute-done.3.refs_1_), channel_id=1, source_target_pairs={{0,1},{1,2},{2,3},{3,0},{4,5},{5,6},{6,7},{7,4},{8,9},{9,10},{10,1... | collective-permute-start | bytes 1572872 | tf_op jit(solution)/shard_map/ppermute | solution.py:27
  54.8 25.3 %collective-permute-start.9 = (bf16[16,2,16,256]{3,2,1,0:T(8,128)(2,1)S(1)}, bf16[16,2,16,256]{3,2,1,0:T(8,128)(2,1)S(1)}, u32[]{:S(2)}, u32[]{:S(2)}) collective-permute-start(bf16[16,2,16,256]{3,2,1,0:T(8,128)(2,1)S(1)} %slice.28), channel_id=1, source_target_pairs={{0,1},{1,2},{2,3},{3,0},{4,5},{5,6},{6,7},{7,4},{8,9},{9,10},{10,1... | collective-permute-start | bytes 786440 | tf_op jit(solution)/shard_map/ppermute | solution.py:27
  57.4 15.7 %copy-start.3 = (bf16[32,2,16,256]{3,2,1,0:T(8,128)(2,1)}, bf16[32,2,16,256]{3,2,1,0:T(8,128)(2,1)S(1)}, u32[]{:S(2)}) copy-start(bf16[32,2,16,256]{3,2,1,0:T(8,128)(2,1)S(1)} %collective-permute-done.7.refs_1_) | copy-start | bytes 1572868
  57.4 22.6 %collective-permute-start.10 = (bf16[16,2,16,256]{3,2,1,0:T(8,128)(2,1)S(1)}, bf16[16,2,16,256]{3,2,1,0:T(8,128)(2,1)}, u32[]{:S(2)}, u32[]{:S(2)}) collective-permute-start(bf16[16,2,16,256]{3,2,1,0:T(8,128)(2,1)S(1)} %slice.29), channel_id=1, source_target_pairs={{0,3},{1,0},{2,1},{3,2},{4,7},{5,4},{6,5},{7,6},{8,11},{9,8},{10,9... | collective-permute-start | bytes 786440 | tf_op jit(solution)/shard_map/ppermute | solution.py:27
  87.1 7.2 %copy-start.27 = (bf16[32,16,256]{2,1,0:T(8,128)(2,1)S(1)}, bf16[32,16,256]{2,1,0:T(8,128)(2,1)}, u32[]{:S(2)}) copy-start(bf16[32,16,256]{2,1,0:T(8,128)(2,1)} %get-tuple-element.113) | copy-start | bytes 786436
  87.1 11.1 %copy-start.26 = (bf16[32,16,256]{2,1,0:T(8,128)(2,1)S(1)}, bf16[32,16,256]{2,1,0:T(8,128)(2,1)}, u32[]{:S(2)}) copy-start(bf16[32,16,256]{2,1,0:T(8,128)(2,1)} %get-tuple-element.114) | copy-start | bytes 786436
  87.1 11.8 %copy-start.25 = (bf16[32,16,256]{2,1,0:T(8,128)(2,1)S(1)}, bf16[32,16,256]{2,1,0:T(8,128)(2,1)}, u32[]{:S(2)}) copy-start(bf16[32,16,256]{2,1,0:T(8,128)(2,1)} %get-tuple-element.115) | copy-start | bytes 786436
  87.1 14.9 %copy-start.12 = (bf16[128,256]{1,0:T(8,128)(2,1)S(1)}, bf16[128,256]{1,0:T(8,128)(2,1)}, u32[]{:S(2)}) copy-start(bf16[128,256]{1,0:T(8,128)(2,1)} %param.21) | copy-start | bytes 196612
  91.5 6.6 %collective-permute-start.18 = (bf16[32,16,256]{2,1,0:T(8,128)(2,1)}, bf16[32,16,256]{2,1,0:T(8,128)(2,1)S(1)}, u32[]{:S(2)}, u32[]{:S(2)}) collective-permute-start(bf16[32,16,256]{2,1,0:T(8,128)(2,1)} %get-tuple-element.116), channel_id=1, source_target_pairs={{0,1},{1,2},{2,3},{3,0},{4,5},{5,6},{6,7},{7,4},{8,9},{9,10},{10,1... | collective-permute-start | bytes 786440 | tf_op jit(solution)/shard_map/ppermute | solution.py:27
  91.5 7.4 %collective-permute-start.19 = (bf16[32,16,256]{2,1,0:T(8,128)(2,1)}, bf16[32,16,256]{2,1,0:T(8,128)(2,1)S(1)}, u32[]{:S(2)}, u32[]{:S(2)}) collective-permute-start(bf16[32,16,256]{2,1,0:T(8,128)(2,1)} %get-tuple-element.117), channel_id=1, source_target_pairs={{0,3},{1,0},{2,1},{3,2},{4,7},{5,4},{6,5},{7,6},{8,11},{9,8},{10,9... | collective-permute-start | bytes 786440 | tf_op jit(solution)/shard_map/ppermute | solution.py:27
  94.2 7.9 %collective-permute-start.20 = (bf16[32,16,256]{2,1,0:T(8,128)(2,1)}, bf16[32,16,256]{2,1,0:T(8,128)(2,1)S(1)}, u32[]{:S(2)}, u32[]{:S(2)}) collective-permute-start(bf16[32,16,256]{2,1,0:T(8,128)(2,1)} %get-tuple-element.118), channel_id=1, source_target_pairs={{0,8},{8,0},{16,24},{24,16},{1,9},{9,1},{17,25},{25,17},{2,10},{10... | collective-permute-start | bytes 786440 | tf_op jit(solution)/shard_map/ppermute | solution.py:31
  94.2 9.7 %collective-permute-start.14 = (bf16[32,16,256]{2,1,0:T(8,128)(2,1)S(1)}, bf16[32,16,256]{2,1,0:T(8,128)(2,1)S(1)}, u32[]{:S(2)}, u32[]{:S(2)}) collective-permute-start(bf16[32,16,256]{2,1,0:T(8,128)(2,1)S(1)} %copy-done.28), channel_id=1, source_target_pairs={{0,9},{1,10},{2,11},{3,8},{8,1},{9,2},{10,3},{11,0},{16,25},{17,26... | collective-permute-start | bytes 786440 | tf_op jit(solution)/shard_map/ppermute | solution.py:36
  94.2 10.7 %collective-permute-start.15 = (bf16[32,16,256]{2,1,0:T(8,128)(2,1)S(1)}, bf16[32,16,256]{2,1,0:T(8,128)(2,1)S(1)}, u32[]{:S(2)}, u32[]{:S(2)}) collective-permute-start(bf16[32,16,256]{2,1,0:T(8,128)(2,1)S(1)} %copy-done.27), channel_id=1, source_target_pairs={{0,11},{1,8},{2,9},{3,10},{8,3},{9,0},{10,1},{11,2},{16,27},{17,24... | collective-permute-start | bytes 786440 | tf_op jit(solution)/shard_map/ppermute | solution.py:36
  98.2 10.9 %collective-permute-start.16 = (bf16[32,16,256]{2,1,0:T(8,128)(2,1)S(1)}, bf16[32,16,256]{2,1,0:T(8,128)(2,1)S(1)}, u32[]{:S(2)}, u32[]{:S(2)}) collective-permute-start(bf16[32,16,256]{2,1,0:T(8,128)(2,1)S(1)} %copy-done.26), channel_id=1, source_target_pairs={{0,2},{1,3},{2,0},{3,1},{4,6},{5,7},{6,4},{7,5},{8,10},{9,11},{10,... | collective-permute-start | bytes 786440 | tf_op jit(solution)/shard_map/ppermute | solution.py:27
  98.9 15.1 %collective-permute-start.17 = (bf16[32,16,256]{2,1,0:T(8,128)(2,1)S(1)}, bf16[32,16,256]{2,1,0:T(8,128)(2,1)S(1)}, u32[]{:S(2)}, u32[]{:S(2)}) collective-permute-start(bf16[32,16,256]{2,1,0:T(8,128)(2,1)S(1)} %copy-done.25), channel_id=1, source_target_pairs={{0,10},{1,11},{2,8},{3,9},{8,2},{9,3},{10,0},{11,1},{16,26},{17,27... | collective-permute-start | bytes 786440 | tf_op jit(solution)/shard_map/ppermute | solution.py:36
  102.1 21.7 %collective-permute-start.24 = (f32[2,128]{1,0:T(2,128)S(1)}, f32[2,128]{1,0:T(2,128)S(1)}, u32[]{:S(2)}, u32[]{:S(2)}) collective-permute-start(f32[2,128]{1,0:T(2,128)S(1)} %pad_maximum_fusion), channel_id=1, source_target_pairs={{0,1},{1,2},{2,3},{3,0},{4,5},{5,6},{6,7},{7,4},{8,9},{9,10},{10,1... | collective-permute-start | bytes 3080 | tf_op jit(solution)/shard_map/ppermute | solution.py:27
  103.9 19.9 %collective-permute-start.25 = (f32[2,128]{1,0:T(2,128)S(1)}, f32[2,128]{1,0:T(2,128)S(1)}, u32[]{:S(2)}, u32[]{:S(2)}) collective-permute-start(f32[2,128]{1,0:T(2,128)S(1)} %pad_maximum_fusion), channel_id=1, source_target_pairs={{0,3},{1,0},{2,1},{3,2},{4,7},{5,4},{6,5},{7,6},{8,11},{9,8},{10,9... | collective-permute-start | bytes 3080 | tf_op jit(solution)/shard_map/ppermute | solution.py:27
  104.9 18.9 %collective-permute-start.26 = (f32[2,128]{1,0:T(2,128)S(1)}, f32[2,128]{1,0:T(2,128)S(1)}, u32[]{:S(2)}, u32[]{:S(2)}) collective-permute-start(f32[2,128]{1,0:T(2,128)S(1)} %pad_maximum_fusion), channel_id=1, source_target_pairs={{0,2},{1,3},{2,0},{3,1},{4,6},{5,7},{6,4},{7,5},{8,10},{9,11},{10,... | collective-permute-start | bytes 3080 | tf_op jit(solution)/shard_map/ppermute | solution.py:27
  116.0 18.2 %all-to-all-start.1 = ((bf16[32,16,256]{2,1,0:T(8,128)(2,1)}), bf16[32,16,256]{2,1,0:T(8,128)(2,1)S(1)}, u32[]{:S(2)}, u32[]{:S(2)}) async-start(bf16[32,16,256]{2,1,0:T(8,128)(2,1)} %add_convert_fusion.1), calls=%async_computation.1 | async-start | bytes 524288 | tf_op jit(solution)/shard_map/all_to_all | solution.py:419
  136.8 5.5 %collective-permute-start.21 = (bf16[128,512]{1,0:T(8,128)(2,1)}, bf16[128,512]{1,0:T(8,128)(2,1)S(1)}, u32[]{:S(2)}, u32[]{:S(2)}) collective-permute-start(bf16[128,512]{1,0:T(8,128)(2,1)} %combine.1.own), channel_id=1, source_target_pairs={{0,1},{1,2},{2,3},{3,0},{4,5},{5,6},{6,7},{7,4},{8,9},{9,10},{10,1... | collective-permute-start | bytes 393224 | tf_op jit(solution)/shard_map/ppermute | solution.py:27
  138.3 5.8 %collective-permute-start.22 = (bf16[128,512]{1,0:T(8,128)(2,1)}, bf16[128,512]{1,0:T(8,128)(2,1)S(1)}, u32[]{:S(2)}, u32[]{:S(2)}) collective-permute-start(bf16[128,512]{1,0:T(8,128)(2,1)} %combine.1.own), channel_id=1, source_target_pairs={{0,2},{1,3},{2,0},{3,1},{4,6},{5,7},{6,4},{7,5},{8,10},{9,11},{10,... | collective-permute-start | bytes 393224 | tf_op jit(solution)/shard_map/ppermute | solution.py:27
  138.7 5.7 %collective-permute-start.23 = (bf16[128,512]{1,0:T(8,128)(2,1)}, bf16[128,512]{1,0:T(8,128)(2,1)S(1)}, u32[]{:S(2)}, u32[]{:S(2)}) collective-permute-start(bf16[128,512]{1,0:T(8,128)(2,1)} %combine.1.own), channel_id=1, source_target_pairs={{0,3},{1,0},{2,1},{3,2},{4,7},{5,4},{6,5},{7,6},{8,11},{9,8},{10,9... | collective-permute-start | bytes 393224 | tf_op jit(solution)/shard_map/ppermute | solution.py:27
  147.9 22.6 %collective-permute-start.27 = (bf16[32,32,256]{2,1,0:T(8,128)(2,1)}, bf16[32,32,256]{2,1,0:T(8,128)(2,1)}, u32[]{:S(2)}, u32[]{:S(2)}) collective-permute-start(bf16[32,32,256]{2,1,0:T(8,128)(2,1)} %get-tuple-element.123), channel_id=1, source_target_pairs={{0,4},{4,0},{1,5},{5,1},{2,6},{6,2},{3,7},{7,3},{8,12},{12,8},{9,1... | collective-permute-start | bytes 1572872 | tf_op jit(solution)/shard_map/ppermute | solution.py:40
  162.8 7.7 %copy-start.15 = (bf16[32,32,256]{2,1,0:T(8,128)(2,1)S(1)}, bf16[32,32,256]{2,1,0:T(8,128)(2,1)}, u32[]{:S(2)}) copy-start(bf16[32,32,256]{2,1,0:T(8,128)(2,1)} %get-tuple-element.122) | copy-start | bytes 1572868
  169.9 18.8 %collective-permute-start.11 = (bf16[224,2048]{1,0:T(8,128)(2,1)}, bf16[224,2048]{1,0:T(8,128)(2,1)S(1)}, u32[]{:S(2)}, u32[]{:S(2)}) collective-permute-start(bf16[224,2048]{1,0:T(8,128)(2,1)} %get-tuple-element.105), channel_id=1, source_target_pairs={{0,4},{4,0},{1,5},{5,1},{2,6},{6,2},{3,7},{7,3},{8,12},{12,8},{9,1... | collective-permute-start | bytes 2752520 | tf_op jit(solution)/shard_map/ppermute | solution.py:40
  169.9 18.8 %collective-permute-start.12 = (bf16[224,2048]{1,0:T(8,128)(2,1)}, bf16[224,2048]{1,0:T(8,128)(2,1)S(1)}, u32[]{:S(2)}, u32[]{:S(2)}) collective-permute-start(bf16[224,2048]{1,0:T(8,128)(2,1)} %get-tuple-element.106), channel_id=1, source_target_pairs={{0,4},{4,0},{1,5},{5,1},{2,6},{6,2},{3,7},{7,3},{8,12},{12,8},{9,1... | collective-permute-start | bytes 2752520 | tf_op jit(solution)/shard_map/ppermute | solution.py:40
  170.4 18.3 %collective-permute-start.13 = (bf16[224,2048]{1,0:T(8,128)(2,1)}, bf16[224,2048]{1,0:T(8,128)(2,1)S(1)}, u32[]{:S(2)}, u32[]{:S(2)}) collective-permute-start(bf16[224,2048]{1,0:T(8,128)(2,1)} %get-tuple-element.107), channel_id=1, source_target_pairs={{0,4},{4,0},{1,5},{5,1},{2,6},{6,2},{3,7},{7,3},{8,12},{12,8},{9,1... | collective-permute-start | bytes 2752520 | tf_op jit(solution)/shard_map/ppermute | solution.py:40
  174.9 8.1 %copy-start.24 = (f32[8,128]{1,0:T(8,128)S(1)}, f32[8,128]{1,0:T(8,128)}, u32[]{:S(2)}) copy-start(f32[8,128]{1,0:T(8,128)} %get-tuple-element.127) | copy-start | bytes 12292
  174.9 3.9 %collective-permute-start.28 = (f32[8,128]{1,0:T(8,128)}, f32[8,128]{1,0:T(8,128)S(1)}, u32[]{:S(2)}, u32[]{:S(2)}) collective-permute-start(f32[8,128]{1,0:T(8,128)} %get-tuple-element.127), channel_id=1, source_target_pairs={{0,1},{1,2},{2,3},{3,0},{4,5},{5,6},{6,7},{7,4},{8,9},{9,10},{10,1... | collective-permute-start | bytes 12296 | tf_op jit(solution)/shard_map/ppermute | solution.py:27
  174.9 7.8 %collective-permute-start.29 = (f32[8,128]{1,0:T(8,128)}, f32[8,128]{1,0:T(8,128)S(1)}, u32[]{:S(2)}, u32[]{:S(2)}) collective-permute-start(f32[8,128]{1,0:T(8,128)} %get-tuple-element.127), channel_id=1, source_target_pairs={{0,3},{1,0},{2,1},{3,2},{4,7},{5,4},{6,5},{7,6},{8,11},{9,8},{10,9... | collective-permute-start | bytes 12296 | tf_op jit(solution)/shard_map/ppermute | solution.py:27
  178.8 4.2 %collective-permute-start.30 = (f32[8,128]{1,0:T(8,128)}, f32[8,128]{1,0:T(8,128)S(1)}, u32[]{:S(2)}, u32[]{:S(2)}) collective-permute-start(f32[8,128]{1,0:T(8,128)} %get-tuple-element.127), channel_id=1, source_target_pairs={{0,2},{1,3},{2,0},{3,1},{4,6},{5,7},{6,4},{7,5},{8,10},{9,11},{10,... | collective-permute-start | bytes 12296 | tf_op jit(solution)/shard_map/ppermute | solution.py:27
  178.8 18.9 %all-to-all-start.2 = ((bf16[32,32,256]{2,1,0:T(8,128)(2,1)}), bf16[32,32,256]{2,1,0:T(8,128)(2,1)S(1)}, u32[]{:S(2)}, u32[]{:S(2)}) async-start(bf16[32,32,256]{2,1,0:T(8,128)(2,1)} %add_convert_fusion), calls=%async_computation.2 | async-start | bytes 1048576 | tf_op jit(solution)/shard_map/all_to_all | solution.py:444
  184.0 10.5 %collective-permute-start.31 = (bf16[30,256]{1,0:T(8,128)(2,1)S(1)}, bf16[30,256]{1,0:T(8,128)(2,1)S(1)}, u32[]{:S(2)}, u32[]{:S(2)}) collective-permute-start(bf16[30,256]{1,0:T(8,128)(2,1)S(1)} %slice.30), channel_id=1, source_target_pairs={{4,0},{8,4},{12,8},{16,12},{20,16},{24,20},{28,24},{32,28},{36,32}... | collective-permute-start | bytes 46088 | tf_op jit(solution)/shard_map/ppermute | solution.py:453
  (16 other events, 30.3 us)
where the time goes:
time: 202 us; the launch traced here: 198 us
  starting transfers between devices  77 us (38%)
  waiting for transfers between devices  57 us (28%)
  Pallas kernels  49.9 us (25%)
  other arithmetic  7.35 us (4%)
  local copies, waits for them, and re-layouts  5.66 us (3%)
    ppermute x18, waiting for transfers between devices, to_y(): return lax.ppermute(v, 'y', [(i, (i + d) % NY) for i in range(NY)])  24.1 us
    ppermute x18, starting transfers between devices, to_y(): return lax.ppermute(v, 'y', [(i, (i + d) % NY) for i in range(NY)])  22.6 us
    ppermute x7, starting transfers between devices, to_c(): return lax.ppermute(v, 'c', [(0, 1), (1, 0)])  17 us
    all_to_all x1, starting transfers between devices, step(): lax.all_to_all(send.reshape(ZX, 2, CAP, 256), ('z', 'x'), 0, 0, tiled=True)  11.9 us
    pallas_call x2, Pallas kernels, stage_pass(): pl.pallas_call(body, out_shape=(jax.ShapeDtypeStruct((ZX * CAP, width), B...  11.8 us
    all_to_all x1, waiting for transfers between devices, step(): returned = lax.all_to_all(total, ('z', 'x'), 0, 0, tiled=True)  10.3 us
    all_to_all x1, starting transfers between devices, step(): returned = lax.all_to_all(total, ('z', 'x'), 0, 0, tiled=True)  7.84 us
    pallas_call x1, Pallas kernels, expert_weights_pass(): pl.pallas_call(weights_body, out_shape=(out,) * 6, in_specs=[VMEM] * 9, o...  7.12 us
  transfers between devices with their start and end apart: 35, of which 19 were waited for; matrix products, arithmetic and copies ran while one was open for 4% of the time, Pallas kernels for 16%

commit v1 on v0

--- a/solution.py
+++ b/solution.py
@@ -17,6 +17,8 @@
 BF16 = jnp.bfloat16
 
 
+BIG = pltpu.CompilerParams(vmem_limit_bytes=20 * 2**20)
+SMALL = pltpu.CompilerParams(vmem_limit_bytes=10 * 2**20)
 VMEM = pl.BlockSpec(memory_space=pltpu.VMEM)
 HBM = pl.BlockSpec(memory_space=pl.ANY)
 CONTRACT_FIRST = (((0,), (0,)), ((), ()))
@@ -29,11 +31,6 @@
 
 def to_x(v):
     return lax.ppermute(v, "x", [(i, i ^ 1) for i in range(NX)])
-
-
-def to_xy(v, d):
-    pairs = [(x * NY + i, (x ^ 1) * NY + (i + d) % NY) for x in range(NX) for i in range(NY)]
-    return lax.ppermute(v, ("x", "y"), pairs)
 
 
 def to_c(v):
@@ -151,6 +148,7 @@
         out_shape=out * 3,
         in_specs=[VMEM] * 6,
         out_specs=(VMEM,) * 9,
+        compiler_params=BIG,
         name="weights_in_order",
     )(*flat)
     return [(res[s], res[3 + s], res[6 + s]) for s in range(3)]
@@ -186,6 +184,7 @@
         in_specs=[VMEM] * (n + 3 + len(before)),
         out_specs=(VMEM,) * 5,
         input_output_aliases={n + 3 + i: 2 + i for i in range(len(before))},
+        compiler_params=BIG,
     )(*pieces, *weights, *before)
 
 
@@ -203,8 +202,8 @@
         grad[...] = part.astype(BF16).reshape(ZX, CAP, 256)
 
 
-FAR = (5, 4, 6, 7)
-NEAR = (2, 1, 3, 0)
+FAR = (5, 4, 7, 3)
+NEAR = (2, 1, 6, 0)
 
 
 def last_body(*refs):
@@ -240,6 +239,7 @@
         + (jax.ShapeDtypeStruct((ZX, CAP, 256), BF16),) * 4,
         in_specs=[VMEM] * 12,
         out_specs=(VMEM,) * 9,
+        compiler_params=BIG,
         name="last_stage",
     )(*pieces, *gate_w, *up_w, down_w, *before)
 
@@ -254,8 +254,25 @@
         out_shape=(jax.ShapeDtypeStruct((ZX, CAP, 256), BF16),) * 4,
         in_specs=[VMEM] * 8,
         out_specs=(VMEM,) * 4,
+        compiler_params=BIG,
         name="near_rows",
     )(d_gate, d_up, *gate_w, *up_w)
+
+
+def add_up(parts):
+    def body(*refs):
+        total = refs[0][...].astype(F32)
+        for part in refs[1:-1]:
+            total = total + part[...].astype(F32)
+        refs[-1][...] = total.astype(BF16)
+
+    return pl.pallas_call(
+        body,
+        out_shape=jax.ShapeDtypeStruct((ZX, CAP, 256), BF16),
+        in_specs=[VMEM] * len(parts),
+        out_specs=VMEM,
+        compiler_params=SMALL,
+    )(*parts)
 
 
 def weights_body(*refs):
@@ -284,6 +301,7 @@
         in_specs=[VMEM] * 9,
         out_specs=(VMEM,) * 6,
         scratch_shapes=[pltpu.VMEM((448, ZX * CAP), BF16)],
+        compiler_params=BIG,
         name="expert_weights",
     )(*rows, *cots, act, d_gate, d_up)
 
@@ -301,6 +319,7 @@
         out_shape=(out,) * 3,
         in_specs=[VMEM] * 6,
         out_specs=(VMEM,) * 3,
+        compiler_params=BIG,
         name="finish",
     )(*own, *others)
 
@@ -319,6 +338,7 @@
         out_shape=jax.ShapeDtypeStruct(cot.shape, BF16),
         in_specs=[VMEM] * 3,
         out_specs=VMEM,
+        compiler_params=SMALL,
         name="combine",
     )(returned, places, cot)
 
@@ -346,6 +366,7 @@
         in_specs=[VMEM] * 5,
         out_specs=(VMEM,) * 3,
         scratch_shapes=[pltpu.VMEM((ZX, 2, 32, 256), BF16)],
+        compiler_params=SMALL,
         name="proj",
     )(*pieces, mixed)
 
@@ -371,6 +392,7 @@
         ),
         in_specs=[VMEM] * 4,
         out_specs=(VMEM,) * 2,
+        compiler_params=SMALL,
         name="channels",
     )(resid, out_proj, normed, gain)
 
@@ -406,14 +428,17 @@
     third = gather_third(second)
     rows1, cots1, *sums = stage_pass(1, second, ordered[1], sums)
     rows2, cots2, act, d_gate, d_up, *far = last_pass(third, gate_w, up_w, down_w[2], sums)
-    far = (to_xy(far[0], 1), to_xy(far[1], -1), to_y(far[2], 2), to_xy(far[3], 2))
+    side = (to_y(far[0], 1), to_y(far[1], -1), to_x(far[2]))
     near = near_pass(d_gate, d_up, gate_w, up_w)
-    near = (near[3], to_y(near[0], 1), to_y(near[1], -1), to_x(near[2]))
+    near_arrived = (to_y(near[0], 1), to_y(near[1], -1))
+    beside = add_up((far[3], side[0], side[1]))
+    opposite = add_up((near[2], side[2]))
+    last_arrived = (to_x(beside), to_y(opposite, 2))
     weight_grads = expert_weights_pass(
         (rows0, rows1, rows2), (cots0, cots1, cots2), act, d_gate, d_up
     )
-    total = near[0].astype(F32)
-    for part in (*far, *near[1:]):
+    total = near[3].astype(F32)
+    for part in (*near_arrived, *last_arrived):
         total = total + part.astype(F32)
     total = total.astype(BF16)
     returned = lax.all_to_all(total, ("z", "x"), 0, 0, tiled=True)

time: 202 us -> 172 us (0.85)
  Pallas kernels: 49.9 us -> 20.7 us
  local copies, waits for them, and re-layouts: 5.66 us -> 16.6 us
  starting transfers between devices: 77 us -> 71.8 us
  other arithmetic: 7.35 us -> 3.71 us
  waiting for transfers between devices: 57 us -> 54.3 us
    unnamed x58 -> x90, local copies, waits for them, and re-layouts: 5.62 us -> 16.6 us
    pallas_call x2, Pallas kernels: 11.8 us -> 4.29 us  [stage_pass(): pl.pallas_call(body, out_shape=(jax.ShapeDtypeStruct((ZX * CAP, width), B...]
    ppermute x3 -> x0, waiting for transfers between devices: 6.76 us -> none  [to_xy(): return lax.ppermute(v, ('x', 'y'), pairs)]
    ppermute x3 -> x0, starting transfers between devices: 6.61 us -> none  [to_xy(): return lax.ppermute(v, ('x', 'y'), pairs)]
    pallas_call x1, Pallas kernels: 5.79 us -> 0.81 us  [weights_in_order(): pl.pallas_call(weights_in_order_body, out_shape=out * 3, in_specs=[VMEM]...]
    ppermute x18 -> x20, waiting for transfers between devices: 24.1 us -> 28.2 us  [to_y(): return lax.ppermute(v, 'y', [(i, (i + d) % NY) for i in range(NY)])]
    pallas_call x1, Pallas kernels: 6.34 us -> 2.37 us  [last_pass(): pl.pallas_call(last_body, out_shape=(jax.ShapeDtypeStruct((n, 256), BF16)...]
    ppermute x7, starting transfers between devices: 17 us -> 13.2 us  [to_c(): return lax.ppermute(v, 'c', [(0, 1), (1, 0)])]
  transfers between devices with their start and end apart: 35 -> 35, of which waited for: 19 -> 14; matrix products, arithmetic and copies ran while one was open for 4% -> 2% of each run, Pallas kernels for 16% -> 9%
where the time goes in v1:
time: 172 us; the launch traced here: 169 us
  starting transfers between devices  71.8 us (42%)
  waiting for transfers between devices  54.3 us (32%)
  Pallas kernels  20.7 us (12%)
  local copies, waits for them, and re-layouts  16.6 us (10%)
  other arithmetic  3.71 us (2%)
    ppermute x20, waiting for transfers between devices, to_y(): return lax.ppermute(v, 'y', [(i, (i + d) % NY) for i in range(NY)])  28.2 us
    ppermute x20, starting transfers between devices, to_y(): return lax.ppermute(v, 'y', [(i, (i + d) % NY) for i in range(NY)])  24.7 us
    unnamed x90, local copies, waits for them, and re-layouts  16.6 us
    ppermute x7, starting transfers between devices, to_c(): return lax.ppermute(v, 'c', [(0, 1), (1, 0)])  13.2 us
    all_to_all x1, starting transfers between devices, step(): lax.all_to_all(send.reshape(ZX, 2, CAP, 256), ('z', 'x'), 0, 0, tiled=True)  12 us
    all_to_all x1, waiting for transfers between devices, step(): returned = lax.all_to_all(total, ('z', 'x'), 0, 0, tiled=True)  10.3 us
    all_to_all x1, starting transfers between devices, step(): returned = lax.all_to_all(total, ('z', 'x'), 0, 0, tiled=True)  9.56 us
    ppermute x4, waiting for transfers between devices, to_x(): return lax.ppermute(v, 'x', [(i, i ^ 1) for i in range(NX)])  6.19 us
  transfers between devices with their start and end apart: 35, of which 14 were waited for; matrix products, arithmetic and copies ran while one was open for 2% of the time, Pallas kernels for 9%

profile of v1, /device:TPU:1, one launch (start us, length us, event | category | flops | bytes accessed | tf_op | source)
XLA Modules:
  0.0 168.8 jit_solution(3796158624216016978)
XLA Ops:
  0.7 2.9 %prep.1 = (bf16[16,2,2,16,256]{4,3,2,1,0:T(8,128)(2,1)}, bf16[256,128]{1,0:T(8,128)(2,1)}, bf16[128,512]{1,0:T(8,128)(2,1)}) custom-call(s32[2,128]{1,0:T(2,128)} %bitcast.63, f32[2,128]{1,0:T(2,128)} %bitcast.64, bf16[128,2048]{1,0:T(8,128)(2,1)} %all_rows.1, bf16[128,2048]{1,0:T(8,128)(2,1)} %all_cots.1), custom_call_target="tpu_custom_call" | custom-call | tf_op jit(solution)/shard_map/prep/pallas_call | solution.py:92
  3.6 12.0 %all-to-all-start = ((bf16[32,2,16,256]{3,2,1,0:T(8,128)(2,1)}), bf16[32,2,16,256]{3,2,1,0:T(8,128)(2,1)}, u32[]{:S(2)}, u32[]{:S(2)}) async-start(bf16[32,2,16,256]{3,2,1,0:T(8,128)(2,1)} %bitcast.58), calls=%async_computation | async-start | bytes 1048576 | tf_op jit(solution)/shard_map/all_to_all | solution.py:420
  15.6 1.0 collective-permute-start
  17.2 1.6 collective-permute-done.refs_1_
  18.7 1.3 collective-permute-done.1.refs_3_
  20.1 1.3 collective-permute-done.2.refs_5_
  21.4 1.2 copy-done.13
  22.6 1.2 copy-done.15
  23.7 1.2 copy-done.16
  28.9 3.0 %all-to-all-done.refs_0_ = bf16[32,2,16,256]{3,2,1,0:T(8,128)(2,1)} async-done(((bf16[32,2,16,256]{3,2,1,0:T(8,128)(2,1)}), bf16[32,2,16,256]{3,2,1,0:T(8,128)(2,1)}, u32[]{:S(2)}, u32[]{:S(2)}) %all-to-all-start) | async-done | bytes 524320 | tf_op jit(solution)/shard_map/all_to_all | solution.py:420
  31.9 1.3 collective-permute-start.3
  33.2 1.0 collective-permute-start.5
  34.2 10.3 %collective-permute-done.3.refs_1_ = bf16[32,2,16,256]{3,2,1,0:T(8,128)(2,1)S(1)} collective-permute-done((bf16[32,2,16,256]{3,2,1,0:T(8,128)(2,1)}, bf16[32,2,16,256]{3,2,1,0:T(8,128)(2,1)S(1)}, u32[]{:S(2)}, u32[]{:S(2)}) %collective-permute-start.3) | collective-permute-done | bytes 524320 | tf_op jit(solution)/shard_map/ppermute | solution.py:29
  44.5 1.5 collective-permute-start.6
  45.9 1.4 collective-permute-start.7
  47.8 1.0 collective-permute-start.8
  48.8 6.2 %collective-permute-done.6.refs_0_ = bf16[32,2,16,256]{3,2,1,0:T(8,128)(2,1)S(1)} collective-permute-done((bf16[32,2,16,256]{3,2,1,0:T(8,128)(2,1)S(1)}, bf16[32,2,16,256]{3,2,1,0:T(8,128)(2,1)S(1)}, u32[]{:S(2)}, u32[]{:S(2)}) %collective-permute-start.6) | collective-permute-done | bytes 524320 | tf_op jit(solution)/shard_map/ppermute | solution.py:33
  55.0 2.6 %collective-permute-start.9 = (bf16[16,2,16,256]{3,2,1,0:T(8,128)(2,1)S(1)}, bf16[16,2,16,256]{3,2,1,0:T(8,128)(2,1)S(1)}, u32[]{:S(2)}, u32[]{:S(2)}) collective-permute-start(bf16[16,2,16,256]{3,2,1,0:T(8,128)(2,1)S(1)} %slice.28), channel_id=1, source_target_pairs={{0,1},{1,2},{2,3},{3,0},{4,5},{5,6},{6,7},{7,4},{8,9},{9,10},{10,1... | collective-permute-start | bytes 786440 | tf_op jit(solution)/shard_map/ppermute | solution.py:29
  57.7 1.5 collective-permute-start.10
  59.2 8.4 %collective-permute-done.4.refs_2_ = bf16[32,2,16,256]{3,2,1,0:T(8,128)(2,1)S(1)} collective-permute-done((bf16[32,2,16,256]{3,2,1,0:T(8,128)(2,1)}, bf16[32,2,16,256]{3,2,1,0:T(8,128)(2,1)S(1)}, u32[]{:S(2)}, u32[]{:S(2)}) %collective-permute-start.4) | collective-permute-done | bytes 524320 | tf_op jit(solution)/shard_map/ppermute | solution.py:29
  67.6 2.8 %shard_map.172 = (bf16[512,1024]{1,0:T(8,128)(2,1)S(1)}, bf16[512,1024]{1,0:T(8,128)(2,1)S(1)}, f32[512,448]{1,0:T(8,128)S(1)}, f32[512,448]{1,0:T(8,128)S(1)}, f32[512,448]{1,0:T(8,128)S(1)}) custom-call(bf16[32,2,16,256]{3,2,1,0:T(8,128)(2,1)} %all-to-all-done.refs_0_, bf16[32,2,16,256]{3,2,1,0:T(8,128)(2,1)S(1)} %collective-permute-done.3.refs_1_, ...), custom_call_target="tpu_custom_call" | custom-call | tf_op jit(solution)/shard_map/pallas_call | solution.py:180
  70.5 1.4 shard_map.173
  73.8 2.4 %last_stage.1 = (bf16[512,256]{1,0:T(8,128)(2,1)S(1)}, bf16[512,256]{1,0:T(8,128)(2,1)S(1)}, bf16[512,448]{1,0:T(8,128)(2,1)S(1)}, bf16[512,448]{1,0:T(8,128)(2,...) custom-call(bf16[16,2,16,256]{3,2,1,0:T(8,128)(2,1)S(1)} %collective, ...), custom_call_target="tpu_custom_call" | custom-call | tf_op jit(solution)/shard_map/last_stage/pallas_call | solution.py:235
  76.3 2.7 %collective-permute-start.17 = (bf16[32,16,256]{2,1,0:T(8,128)(2,1)S(1)}, bf16[32,16,256]{2,1,0:T(8,128)(2,1)S(1)}, u32[]{:S(2)}, u32[]{:S(2)}) collective-permute-start(bf16[32,16,256]{2,1,0:T(8,128)(2,1)S(1)} %get-tuple-element.116), channel_id=1, source_target_pairs={{0,3},{1,0},{2,1},{3,2},{4,7},{5,4},{6,5},{7,6},{8,11},{9,8},{10,9... | collective-permute-start | bytes 786440 | tf_op jit(solution)/shard_map/ppermute | solution.py:29
  79.0 1.2 near_rows.1
  80.4 2.7 %collective-permute-start.15 = (bf16[32,16,256]{2,1,0:T(8,128)(2,1)S(1)}, bf16[32,16,256]{2,1,0:T(8,128)(2,1)S(1)}, u32[]{:S(2)}, u32[]{:S(2)}) collective-permute-start(bf16[32,16,256]{2,1,0:T(8,128)(2,1)S(1)} %get-tuple-element.113), channel_id=1, source_target_pairs={{0,3},{1,0},{2,1},{3,2},{4,7},{5,4},{6,5},{7,6},{8,11},{9,8},{10,9... | collective-permute-start | bytes 786440 | tf_op jit(solution)/shard_map/ppermute | solution.py:29
  83.1 1.6 collective-permute-start.18
  86.8 1.8 %collective-permute-start.25 = (f32[2,128]{1,0:T(2,128)S(1)}, f32[2,128]{1,0:T(2,128)S(1)}, u32[]{:S(2)}, u32[]{:S(2)}) collective-permute-start(f32[2,128]{1,0:T(2,128)S(1)} %pad_maximum_fusion), channel_id=1, source_target_pairs={{0,3},{1,0},{2,1},{3,2},{4,7},{5,4},{6,5},{7,6},{8,11},{9,8},{10,9... | collective-permute-start | bytes 3080 | tf_op jit(solution)/shard_map/ppermute | solution.py:29
  89.5 4.9 %collective-permute-done.20 = bf16[32,16,256]{2,1,0:T(8,128)(2,1)S(1)} collective-permute-done((bf16[32,16,256]{2,1,0:T(8,128)(2,1)S(1)}, bf16[32,16,256]{2,1,0:T(8,128)(2,1)S(1)}, u32[]{:S(2)}, u32[]{:S(2)}) %collective-permute-start.20) | collective-permute-done | bytes 262176 | tf_op jit(solution)/shard_map/ppermute | solution.py:29
  95.3 9.6 %all-to-all-start.1 = ((bf16[32,16,256]{2,1,0:T(8,128)(2,1)}), bf16[32,16,256]{2,1,0:T(8,128)(2,1)S(1)}, u32[]{:S(2)}, u32[]{:S(2)}) async-start(bf16[32,16,256]{2,1,0:T(8,128)(2,1)} %add_convert_fusion.1), calls=%async_computation.1 | async-start | bytes 524288 | tf_op jit(solution)/shard_map/all_to_all | solution.py:444
  104.9 10.3 %all-to-all-done.1 = bf16[32,16,256]{2,1,0:T(8,128)(2,1)S(1)} async-done(((bf16[32,16,256]{2,1,0:T(8,128)(2,1)}), bf16[32,16,256]{2,1,0:T(8,128)(2,1)S(1)}, u32[]{:S(2)}, u32[]{:S(2)}) %all-to-all-start.1) | async-done | bytes 262176 | tf_op jit(solution)/shard_map/all_to_all | solution.py:444
  116.2 2.6 %collective-permute-start.22 = (bf16[128,512]{1,0:T(8,128)(2,1)S(1)}, bf16[128,512]{1,0:T(8,128)(2,1)S(1)}, u32[]{:S(2)}, u32[]{:S(2)}) collective-permute-start(bf16[128,512]{1,0:T(8,128)(2,1)S(1)} %combine.1.own), channel_id=1, source_target_pairs={{0,2},{1,3},{2,0},{3,1},{4,6},{5,7},{6,4},{7,5},{8,10},{9,11},{10,... | collective-permute-start | bytes 393224 | tf_op jit(solution)/shard_map/ppermute | solution.py:29
  119.3 1.6 collective-permute-done.21.one
  120.9 1.8 %collective-permute-done.22.two = bf16[128,512]{1,0:T(8,128)(2,1)S(1)} collective-permute-done((bf16[128,512]{1,0:T(8,128)(2,1)S(1)}, bf16[128,512]{1,0:T(8,128)(2,1)S(1)}, u32[]{:S(2)}, u32[]{:S(2)}) %collective-permute-start.22) | collective-permute-done | bytes 131104 | tf_op jit(solution)/shard_map/ppermute | solution.py:29
  123.3 10.9 %collective-permute-start.27 = (bf16[32,32,256]{2,1,0:T(8,128)(2,1)S(1)}, bf16[32,32,256]{2,1,0:T(8,128)(2,1)S(1)}, u32[]{:S(2)}, u32[]{:S(2)}) collective-permute-start(bf16[32,32,256]{2,1,0:T(8,128)(2,1)S(1)} %get-tuple-element.123), channel_id=1, source_target_pairs={{0,4},{4,0},{1,5},{5,1},{2,6},{6,2},{3,7},{7,3},{8,12},{12,8},{9,1... | collective-permute-start | bytes 1572872 | tf_op jit(solution)/shard_map/ppermute | solution.py:37
  134.3 1.1 copy-done.26
  135.4 1.1 copy-done.28
  136.5 1.0 copy-done.32
  138.5 4.3 %expert_weights.1 = (bf16[224,2048]{1,0:T(8,128)(2,1)S(1)}, bf16[224,2048]{1,0:T(8,128)(2,1)S(1)}, bf16[224,2048]{1,0:T(8,128)(2,1)S(1)}, bf16[224,2048]{1,0:T(8...) custom-call(bf16[512,1024]{1,0:T(8,128)(2,1)S(1)} %copy-done.7, bf16[512,768]{1,0:T(8,128)(2,1)S(1)} %copy-done.26, ...), custom_call_target="tpu_custom_call" | custom-call | tf_op jit(solution)/shard_map/expert_weights/pallas_call | solution.py:298
  143.5 1.0 add_convert_fusion
  145.2 2.7 %collective-permute-start.29 = (f32[8,128]{1,0:T(8,128)S(1)}, f32[8,128]{1,0:T(8,128)S(1)}, u32[]{:S(2)}, u32[]{:S(2)}) collective-permute-start(f32[8,128]{1,0:T(8,128)S(1)} %get-tuple-element.127), channel_id=1, source_target_pairs={{0,3},{1,0},{2,1},{3,2},{4,7},{5,4},{6,5},{7,6},{8,11},{9,8},{10,9... | collective-permute-start | bytes 12296 | tf_op jit(solution)/shard_map/ppermute | solution.py:29
  147.9 1.0 collective-permute-done.28
  148.9 3.9 %all-to-all-start.2 = ((bf16[32,32,256]{2,1,0:T(8,128)(2,1)}), bf16[32,32,256]{2,1,0:T(8,128)(2,1)S(1)}, u32[]{:S(2)}, u32[]{:S(2)}) async-start(bf16[32,32,256]{2,1,0:T(8,128)(2,1)} %add_convert_fusion), calls=%async_computation.2 | async-start | bytes 1048576 | tf_op jit(solution)/shard_map/all_to_all | solution.py:469
  153.0 4.4 %collective-permute-start.31 = (bf16[30,256]{1,0:T(8,128)(2,1)S(1)}, bf16[30,256]{1,0:T(8,128)(2,1)S(1)}, u32[]{:S(2)}, u32[]{:S(2)}) collective-permute-start(bf16[30,256]{1,0:T(8,128)(2,1)S(1)} %slice.30), channel_id=1, source_target_pairs={{4,0},{8,4},{12,8},{16,12},{20,16},{24,20},{28,24},{32,28},{36,32}... | collective-permute-start | bytes 46088 | tf_op jit(solution)/shard_map/ppermute | solution.py:478
  158.4 1.2 copy-done.20
  159.5 1.2 copy-done.22
  160.7 3.4 %finish.1 = (bf16[224,2048]{1,0:T(8,128)(2,1)}, bf16[224,2048]{1,0:T(8,128)(2,1)}, bf16[224,2048]{1,0:T(8,128)(2,1)}) custom-call(bf16[224,2048]{1,0:T(8,128)(2,1)S(1)} %get-tuple-element.102.refs_0_, bf16[224,2048]{1,0:T(8,128)(2,1)S(1)} %copy-done.18, bf16[224,2048]{1,0:T(8,128)(2,1)S(1)} %copy-done.20, bf16[224,2048]{1,0:T(8,128)(2,1)S(1)} %copy-done.22, ...), custom_call_target="tpu_custom_call" | custom-call | tf_op jit(solution)/shard_map/finish/pallas_call | solution.py:317
  165.7 2.4 %all-to-all-done.2 = bf16[32,32,256]{2,1,0:T(8,128)(2,1)S(1)} async-done(((bf16[32,32,256]{2,1,0:T(8,128)(2,1)}), bf16[32,32,256]{2,1,0:T(8,128)(2,1)S(1)}, u32[]{:S(2)}, u32[]{:S(2)}) %all-to-all-start.2) | async-done | bytes 524320 | tf_op jit(solution)/shard_map/all_to_all | solution.py:469
  (143 shorter events, 18.8 us)
Async XLA Ops:
  0.6 163.5 %copy-start = (f32[31,256]{1,0:T(8,128)S(1)}, f32[31,256]{1,0:T(8,128)}, u32[]{:S(2)}) copy-start(f32[31,256]{1,0:T(8,128)} %param.24) | copy-start | bytes 95236
  0.6 14.9 %copy-start.12 = (bf16[1,2048,224]{1,2,0:T(8,128)(2,1)S(1)}, bf16[1,2048,224]{1,2,0:T(8,128)(2,1)}, u32[]{:S(2)}) copy-start(bf16[1,2048,224]{1,2,0:T(8,128)(2,1)} %param.17) | copy-start | bytes 2752516
  0.7 16.0 %copy-start.14 = (bf16[1,2048,224]{1,2,0:T(8,128)(2,1)S(1)}, bf16[1,2048,224]{1,2,0:T(8,128)(2,1)}, u32[]{:S(2)}) copy-start(bf16[1,2048,224]{1,2,0:T(8,128)(2,1)} %param.18) | copy-start | bytes 2752516
  3.6 28.3 %all-to-all-start = ((bf16[32,2,16,256]{3,2,1,0:T(8,128)(2,1)}), bf16[32,2,16,256]{3,2,1,0:T(8,128)(2,1)}, u32[]{:S(2)}, u32[]{:S(2)}) async-start(bf16[32,2,16,256]{3,2,1,0:T(8,128)(2,1)} %bitcast.58), calls=%async_computation | async-start | bytes 1048576 | tf_op jit(solution)/shard_map/all_to_all | solution.py:420
  15.6 3.1 %collective-permute-start = (bf16[224,2048]{1,0:T(8,128)(2,1)S(1)}, bf16[224,2048]{1,0:T(8,128)(2,1)S(1)}, u32[]{:S(2)}, u32[]{:S(2)}) collective-permute-start(bf16[224,2048]{1,0:T(8,128)(2,1)S(1)} %bitcast.51), channel_id=1, source_target_pairs={{0,4},{4,0},{1,5},{5,1},{2,6},{6,2},{3,7},{7,3},{8,12},{12,8},{9,1... | collective-permute-start | bytes 2752520 | tf_op jit(solution)/shard_map/ppermute | solution.py:37
  16.6 3.4 %collective-permute-start.1 = (bf16[224,2048]{1,0:T(8,128)(2,1)S(1)}, bf16[224,2048]{1,0:T(8,128)(2,1)S(1)}, u32[]{:S(2)}, u32[]{:S(2)}) collective-permute-start(bf16[224,2048]{1,0:T(8,128)(2,1)S(1)} %bitcast.53), channel_id=1, source_target_pairs={{0,4},{4,0},{1,5},{5,1},{2,6},{6,2},{3,7},{7,3},{8,12},{12,8},{9,1... | collective-permute-start | bytes 2752520 | tf_op jit(solution)/shard_map/ppermute | solution.py:37
  16.8 4.6 %collective-permute-start.2 = (bf16[224,2048]{1,0:T(8,128)(2,1)}, bf16[224,2048]{1,0:T(8,128)(2,1)S(1)}, u32[]{:S(2)}, u32[]{:S(2)}) collective-permute-start(bf16[224,2048]{1,0:T(8,128)(2,1)} %bitcast.55), channel_id=1, source_target_pairs={{0,4},{4,0},{1,5},{5,1},{2,6},{6,2},{3,7},{7,3},{8,12},{12,8},{9,1... | collective-permute-start | bytes 2752520 | tf_op jit(solution)/shard_map/ppermute | solution.py:37
  31.9 35.8 %copy-start.11 = (bf16[448,1024]{1,0:T(8,128)(2,1)S(1)}, bf16[448,1024]{1,0:T(8,128)(2,1)}, u32[]{:S(2)}) copy-start(bf16[448,1024]{1,0:T(8,128)(2,1)} %copy-done.10) | copy-start | bytes 2752516
  31.9 12.6 %collective-permute-start.3 = (bf16[32,2,16,256]{3,2,1,0:T(8,128)(2,1)}, bf16[32,2,16,256]{3,2,1,0:T(8,128)(2,1)S(1)}, u32[]{:S(2)}, u32[]{:S(2)}) collective-permute-start(bf16[32,2,16,256]{3,2,1,0:T(8,128)(2,1)} %all-to-all-done.refs_0_), channel_id=1, source_target_pairs={{0,1},{1,2},{2,3},{3,0},{4,5},{5,6},{6,7},{7,4},{8,9},{9,10},{10,1... | collective-permute-start | bytes 1572872 | tf_op jit(solution)/shard_map/ppermute | solution.py:29
  33.2 12.8 %collective-permute-start.5 = (bf16[32,2,16,256]{3,2,1,0:T(8,128)(2,1)}, bf16[32,2,16,256]{3,2,1,0:T(8,128)(2,1)S(1)}, u32[]{:S(2)}, u32[]{:S(2)}) collective-permute-start(bf16[32,2,16,256]{3,2,1,0:T(8,128)(2,1)} %all-to-all-done.refs_0_), channel_id=1, source_target_pairs={{0,8},{8,0},{16,24},{24,16},{1,9},{9,1},{17,25},{25,17},{2,10},{10... | collective-permute-start | bytes 1572872 | tf_op jit(solution)/shard_map/ppermute | solution.py:33
  44.5 10.5 %collective-permute-start.6 = (bf16[32,2,16,256]{3,2,1,0:T(8,128)(2,1)S(1)}, bf16[32,2,16,256]{3,2,1,0:T(8,128)(2,1)S(1)}, u32[]{:S(2)}, u32[]{:S(2)}) collective-permute-start(bf16[32,2,16,256]{3,2,1,0:T(8,128)(2,1)S(1)} %collective-permute-done.3.refs_1_), channel_id=1, source_target_pairs={{0,8},{8,0},{16,24},{24,16},{1,9},{9,1},{17,25},{25,17},{2,10},{10... | collective-permute-start | bytes 1572872 | tf_op jit(solution)/shard_map/ppermute | solution.py:33
  45.9 11.7 %collective-permute-start.7 = (bf16[32,2,16,256]{3,2,1,0:T(8,128)(2,1)S(1)}, bf16[32,2,16,256]{3,2,1,0:T(8,128)(2,1)S(1)}, u32[]{:S(2)}, u32[]{:S(2)}) collective-permute-start(bf16[32,2,16,256]{3,2,1,0:T(8,128)(2,1)S(1)} %collective-permute-done.5.refs_3_), channel_id=1, source_target_pairs={{0,3},{1,0},{2,1},{3,2},{4,7},{5,4},{6,5},{7,6},{8,11},{9,8},{10,9... | collective-permute-start | bytes 1572872 | tf_op jit(solution)/shard_map/ppermute | solution.py:29
  47.3 20.3 %collective-permute-start.4 = (bf16[32,2,16,256]{3,2,1,0:T(8,128)(2,1)}, bf16[32,2,16,256]{3,2,1,0:T(8,128)(2,1)S(1)}, u32[]{:S(2)}, u32[]{:S(2)}) collective-permute-start(bf16[32,2,16,256]{3,2,1,0:T(8,128)(2,1)} %all-to-all-done.refs_0_), channel_id=1, source_target_pairs={{0,3},{1,0},{2,1},{3,2},{4,7},{5,4},{6,5},{7,6},{8,11},{9,8},{10,9... | collective-permute-start | bytes 1572872 | tf_op jit(solution)/shard_map/ppermute | solution.py:29
  47.8 22.7 %collective-permute-start.8 = (bf16[32,2,16,256]{3,2,1,0:T(8,128)(2,1)S(1)}, bf16[32,2,16,256]{3,2,1,0:T(8,128)(2,1)S(1)}, u32[]{:S(2)}, u32[]{:S(2)}) collective-permute-start(bf16[32,2,16,256]{3,2,1,0:T(8,128)(2,1)S(1)} %collective-permute-done.3.refs_1_), channel_id=1, source_target_pairs={{0,1},{1,2},{2,3},{3,0},{4,5},{5,6},{6,7},{7,4},{8,9},{9,10},{10,1... | collective-permute-start | bytes 1572872 | tf_op jit(solution)/shard_map/ppermute | solution.py:29
  55.0 18.7 %collective-permute-start.9 = (bf16[16,2,16,256]{3,2,1,0:T(8,128)(2,1)S(1)}, bf16[16,2,16,256]{3,2,1,0:T(8,128)(2,1)S(1)}, u32[]{:S(2)}, u32[]{:S(2)}) collective-permute-start(bf16[16,2,16,256]{3,2,1,0:T(8,128)(2,1)S(1)} %slice.28), channel_id=1, source_target_pairs={{0,1},{1,2},{2,3},{3,0},{4,5},{5,6},{6,7},{7,4},{8,9},{9,10},{10,1... | collective-permute-start | bytes 786440 | tf_op jit(solution)/shard_map/ppermute | solution.py:29
  57.7 12.8 %copy-start.30 = (bf16[448,768]{1,0:T(8,128)(2,1)S(1)}, bf16[448,768]{1,0:T(8,128)(2,1)}, u32[]{:S(2)}) copy-start(bf16[448,768]{1,0:T(8,128)(2,1)} %copy-done.29) | copy-start | bytes 2064388
  57.7 16.1 %collective-permute-start.10 = (bf16[16,2,16,256]{3,2,1,0:T(8,128)(2,1)S(1)}, bf16[16,2,16,256]{3,2,1,0:T(8,128)(2,1)S(1)}, u32[]{:S(2)}, u32[]{:S(2)}) collective-permute-start(bf16[16,2,16,256]{3,2,1,0:T(8,128)(2,1)S(1)} %slice.29), channel_id=1, source_target_pairs={{0,3},{1,0},{2,1},{3,2},{4,7},{5,4},{6,5},{7,6},{8,11},{9,8},{10,9... | collective-permute-start | bytes 786440 | tf_op jit(solution)/shard_map/ppermute | solution.py:29
  76.2 6.8 %collective-permute-start.16 = (bf16[32,16,256]{2,1,0:T(8,128)(2,1)S(1)}, bf16[32,16,256]{2,1,0:T(8,128)(2,1)S(1)}, u32[]{:S(2)}, u32[]{:S(2)}) collective-permute-start(bf16[32,16,256]{2,1,0:T(8,128)(2,1)S(1)} %get-tuple-element.115), channel_id=1, source_target_pairs={{0,1},{1,2},{2,3},{3,0},{4,5},{5,6},{6,7},{7,4},{8,9},{9,10},{10,1... | collective-permute-start | bytes 786440 | tf_op jit(solution)/shard_map/ppermute | solution.py:29
  76.3 6.7 %collective-permute-start.17 = (bf16[32,16,256]{2,1,0:T(8,128)(2,1)S(1)}, bf16[32,16,256]{2,1,0:T(8,128)(2,1)S(1)}, u32[]{:S(2)}, u32[]{:S(2)}) collective-permute-start(bf16[32,16,256]{2,1,0:T(8,128)(2,1)S(1)} %get-tuple-element.116), channel_id=1, source_target_pairs={{0,3},{1,0},{2,1},{3,2},{4,7},{5,4},{6,5},{7,6},{8,11},{9,8},{10,9... | collective-permute-start | bytes 786440 | tf_op jit(solution)/shard_map/ppermute | solution.py:29
  79.0 5.7 %collective-permute-start.19 = (bf16[32,16,256]{2,1,0:T(8,128)(2,1)S(1)}, bf16[32,16,256]{2,1,0:T(8,128)(2,1)S(1)}, u32[]{:S(2)}, u32[]{:S(2)}) collective-permute-start(bf16[32,16,256]{2,1,0:T(8,128)(2,1)S(1)} %get-tuple-element.118), channel_id=1, source_target_pairs={{0,8},{8,0},{16,24},{24,16},{1,9},{9,1},{17,25},{25,17},{2,10},{10... | collective-permute-start | bytes 786440 | tf_op jit(solution)/shard_map/ppermute | solution.py:33
  80.3 6.5 %collective-permute-start.14 = (bf16[32,16,256]{2,1,0:T(8,128)(2,1)S(1)}, bf16[32,16,256]{2,1,0:T(8,128)(2,1)S(1)}, u32[]{:S(2)}, u32[]{:S(2)}) collective-permute-start(bf16[32,16,256]{2,1,0:T(8,128)(2,1)S(1)} %get-tuple-element.112), channel_id=1, source_target_pairs={{0,1},{1,2},{2,3},{3,0},{4,5},{5,6},{6,7},{7,4},{8,9},{9,10},{10,1... | collective-permute-start | bytes 786440 | tf_op jit(solution)/shard_map/ppermute | solution.py:29
  80.4 8.2 %collective-permute-start.15 = (bf16[32,16,256]{2,1,0:T(8,128)(2,1)S(1)}, bf16[32,16,256]{2,1,0:T(8,128)(2,1)S(1)}, u32[]{:S(2)}, u32[]{:S(2)}) collective-permute-start(bf16[32,16,256]{2,1,0:T(8,128)(2,1)S(1)} %get-tuple-element.113), channel_id=1, source_target_pairs={{0,3},{1,0},{2,1},{3,2},{4,7},{5,4},{6,5},{7,6},{8,11},{9,8},{10,9... | collective-permute-start | bytes 786440 | tf_op jit(solution)/shard_map/ppermute | solution.py:29
  83.1 6.4 %collective-permute-start.18 = (bf16[32,16,256]{2,1,0:T(8,128)(2,1)S(1)}, bf16[32,16,256]{2,1,0:T(8,128)(2,1)S(1)}, u32[]{:S(2)}, u32[]{:S(2)}) collective-permute-start(bf16[32,16,256]{2,1,0:T(8,128)(2,1)S(1)} %shard_map.174), channel_id=1, source_target_pairs={{0,8},{8,0},{16,24},{24,16},{1,9},{9,1},{17,25},{25,17},{2,10},{10... | collective-permute-start | bytes 786440 | tf_op jit(solution)/shard_map/ppermute | solution.py:33
  84.7 30.5 %copy-start.39 = (bf16[128,512]{1,0:T(8,128)(2,1)S(1)}, bf16[128,512]{1,0:T(8,128)(2,1)}, u32[]{:S(2)}) copy-start(bf16[128,512]{1,0:T(8,128)(2,1)} %get-tuple-element.120.cot) | copy-start | bytes 393220
  84.7 30.5 %copy-start.40 = (bf16[256,128]{1,0:T(8,128)(2,1)S(1)}, bf16[256,128]{1,0:T(8,128)(2,1)}, u32[]{:S(2)}) copy-start(bf16[256,128]{1,0:T(8,128)(2,1)} %get-tuple-element.119.places) | copy-start | bytes 196612
  84.8 9.6 %collective-permute-start.20 = (bf16[32,16,256]{2,1,0:T(8,128)(2,1)S(1)}, bf16[32,16,256]{2,1,0:T(8,128)(2,1)S(1)}, u32[]{:S(2)}, u32[]{:S(2)}) collective-permute-start(bf16[32,16,256]{2,1,0:T(8,128)(2,1)S(1)} %shard_map.175), channel_id=1, source_target_pairs={{0,2},{1,3},{2,0},{3,1},{4,6},{5,7},{6,4},{7,5},{8,10},{9,11},{10,... | collective-permute-start | bytes 786440 | tf_op jit(solution)/shard_map/ppermute | solution.py:29
  85.8 19.0 %collective-permute-start.24 = (f32[2,128]{1,0:T(2,128)S(1)}, f32[2,128]{1,0:T(2,128)S(1)}, u32[]{:S(2)}, u32[]{:S(2)}) collective-permute-start(f32[2,128]{1,0:T(2,128)S(1)} %pad_maximum_fusion), channel_id=1, source_target_pairs={{0,1},{1,2},{2,3},{3,0},{4,5},{5,6},{6,7},{7,4},{8,9},{9,10},{10,1... | collective-permute-start | bytes 3080 | tf_op jit(solution)/shard_map/ppermute | solution.py:29
  86.8 18.1 %collective-permute-start.25 = (f32[2,128]{1,0:T(2,128)S(1)}, f32[2,128]{1,0:T(2,128)S(1)}, u32[]{:S(2)}, u32[]{:S(2)}) collective-permute-start(f32[2,128]{1,0:T(2,128)S(1)} %pad_maximum_fusion), channel_id=1, source_target_pairs={{0,3},{1,0},{2,1},{3,2},{4,7},{5,4},{6,5},{7,6},{8,11},{9,8},{10,9... | collective-permute-start | bytes 3080 | tf_op jit(solution)/shard_map/ppermute | solution.py:29
  88.5 16.3 %collective-permute-start.26 = (f32[2,128]{1,0:T(2,128)S(1)}, f32[2,128]{1,0:T(2,128)S(1)}, u32[]{:S(2)}, u32[]{:S(2)}) collective-permute-start(f32[2,128]{1,0:T(2,128)S(1)} %pad_maximum_fusion), channel_id=1, source_target_pairs={{0,2},{1,3},{2,0},{3,1},{4,6},{5,7},{6,4},{7,5},{8,10},{9,11},{10,... | collective-permute-start | bytes 3080 | tf_op jit(solution)/shard_map/ppermute | solution.py:29
  94.4 39.8 %copy-start.7 = (bf16[512,1024]{1,0:T(8,128)(2,1)S(1)}, bf16[512,1024]{1,0:T(8,128)(2,1)}, u32[]{:S(2)}) copy-start(bf16[512,1024]{1,0:T(8,128)(2,1)} %copy-done.6) | copy-start | bytes 3145732
  94.4 39.8 %copy-start.9 = (bf16[512,1024]{1,0:T(8,128)(2,1)S(1)}, bf16[512,1024]{1,0:T(8,128)(2,1)}, u32[]{:S(2)}) copy-start(bf16[512,1024]{1,0:T(8,128)(2,1)} %copy-done.8) | copy-start | bytes 3145732
  95.3 20.0 %all-to-all-start.1 = ((bf16[32,16,256]{2,1,0:T(8,128)(2,1)}), bf16[32,16,256]{2,1,0:T(8,128)(2,1)S(1)}, u32[]{:S(2)}, u32[]{:S(2)}) async-start(bf16[32,16,256]{2,1,0:T(8,128)(2,1)} %add_convert_fusion.1), calls=%async_computation.1 | async-start | bytes 524288 | tf_op jit(solution)/shard_map/all_to_all | solution.py:444
  115.2 19.0 %copy-start.4 = (bf16[512,448]{1,0:T(8,128)(2,1)S(1)}, bf16[512,448]{1,0:T(8,128)(2,1)}, u32[]{:S(2)}) copy-start(bf16[512,448]{1,0:T(8,128)(2,1)} %copy-done.3) | copy-start | bytes 1376260
  115.5 18.8 %copy-start.2 = (bf16[512,448]{1,0:T(8,128)(2,1)S(1)}, bf16[512,448]{1,0:T(8,128)(2,1)}, u32[]{:S(2)}) copy-start(bf16[512,448]{1,0:T(8,128)(2,1)} %copy-done.1) | copy-start | bytes 1376260
  115.5 5.4 %collective-permute-start.21 = (bf16[128,512]{1,0:T(8,128)(2,1)S(1)}, bf16[128,512]{1,0:T(8,128)(2,1)S(1)}, u32[]{:S(2)}, u32[]{:S(2)}) collective-permute-start(bf16[128,512]{1,0:T(8,128)(2,1)S(1)} %combine.1.own), channel_id=1, source_target_pairs={{0,1},{1,2},{2,3},{3,0},{4,5},{5,6},{6,7},{7,4},{8,9},{9,10},{10,1... | collective-permute-start | bytes 393224 | tf_op jit(solution)/shard_map/ppermute | solution.py:29
  116.2 6.4 %collective-permute-start.22 = (bf16[128,512]{1,0:T(8,128)(2,1)S(1)}, bf16[128,512]{1,0:T(8,128)(2,1)S(1)}, u32[]{:S(2)}, u32[]{:S(2)}) collective-permute-start(bf16[128,512]{1,0:T(8,128)(2,1)S(1)} %combine.1.own), channel_id=1, source_target_pairs={{0,2},{1,3},{2,0},{3,1},{4,6},{5,7},{6,4},{7,5},{8,10},{9,11},{10,... | collective-permute-start | bytes 393224 | tf_op jit(solution)/shard_map/ppermute | solution.py:29
  118.9 3.8 %collective-permute-start.23 = (bf16[128,512]{1,0:T(8,128)(2,1)S(1)}, bf16[128,512]{1,0:T(8,128)(2,1)S(1)}, u32[]{:S(2)}, u32[]{:S(2)}) collective-permute-start(bf16[128,512]{1,0:T(8,128)(2,1)S(1)} %combine.1.own), channel_id=1, source_target_pairs={{0,3},{1,0},{2,1},{3,2},{4,7},{5,4},{6,5},{7,6},{8,11},{9,8},{10,9... | collective-permute-start | bytes 393224 | tf_op jit(solution)/shard_map/ppermute | solution.py:29
  122.7 11.5 %copy-start.34 = (bf16[512,256]{1,0:T(8,128)(2,1)S(1)}, bf16[512,256]{1,0:T(8,128)(2,1)}, u32[]{:S(2)}) copy-start(bf16[512,256]{1,0:T(8,128)(2,1)} %copy-done.33) | copy-start | bytes 786436
  123.3 20.2 %collective-permute-start.27 = (bf16[32,32,256]{2,1,0:T(8,128)(2,1)S(1)}, bf16[32,32,256]{2,1,0:T(8,128)(2,1)S(1)}, u32[]{:S(2)}, u32[]{:S(2)}) collective-permute-start(bf16[32,32,256]{2,1,0:T(8,128)(2,1)S(1)} %get-tuple-element.123), channel_id=1, source_target_pairs={{0,4},{4,0},{1,5},{5,1},{2,6},{6,2},{3,7},{7,3},{8,12},{12,8},{9,1... | collective-permute-start | bytes 1572872 | tf_op jit(solution)/shard_map/ppermute | solution.py:37
  142.8 14.6 %collective-permute-start.11 = (bf16[224,2048]{1,0:T(8,128)(2,1)}, bf16[224,2048]{1,0:T(8,128)(2,1)S(1)}, u32[]{:S(2)}, u32[]{:S(2)}) collective-permute-start(bf16[224,2048]{1,0:T(8,128)(2,1)} %get-tuple-element.105), channel_id=1, source_target_pairs={{0,4},{4,0},{1,5},{5,1},{2,6},{6,2},{3,7},{7,3},{8,12},{12,8},{9,1... | collective-permute-start | bytes 2752520 | tf_op jit(solution)/shard_map/ppermute | solution.py:37
  143.0 15.3 %collective-permute-start.12 = (bf16[224,2048]{1,0:T(8,128)(2,1)}, bf16[224,2048]{1,0:T(8,128)(2,1)}, u32[]{:S(2)}, u32[]{:S(2)}) collective-permute-start(bf16[224,2048]{1,0:T(8,128)(2,1)} %get-tuple-element.106), channel_id=1, source_target_pairs={{0,4},{4,0},{1,5},{5,1},{2,6},{6,2},{3,7},{7,3},{8,12},{12,8},{9,1... | collective-permute-start | bytes 2752520 | tf_op jit(solution)/shard_map/ppermute | solution.py:37
  143.3 15.1 %collective-permute-start.13 = (bf16[224,2048]{1,0:T(8,128)(2,1)}, bf16[224,2048]{1,0:T(8,128)(2,1)}, u32[]{:S(2)}, u32[]{:S(2)}) collective-permute-start(bf16[224,2048]{1,0:T(8,128)(2,1)} %get-tuple-element.107), channel_id=1, source_target_pairs={{0,4},{4,0},{1,5},{5,1},{2,6},{6,2},{3,7},{7,3},{8,12},{12,8},{9,1... | collective-permute-start | bytes 2752520 | tf_op jit(solution)/shard_map/ppermute | solution.py:37
  145.1 13.2 %copy-start.18 = (bf16[224,2048]{1,0:T(8,128)(2,1)S(1)}, bf16[224,2048]{1,0:T(8,128)(2,1)}, u32[]{:S(2)}) copy-start(bf16[224,2048]{1,0:T(8,128)(2,1)} %copy-done.17) | copy-start | bytes 2752516
  145.1 3.7 %collective-permute-start.28 = (f32[8,128]{1,0:T(8,128)S(1)}, f32[8,128]{1,0:T(8,128)S(1)}, u32[]{:S(2)}, u32[]{:S(2)}) collective-permute-start(f32[8,128]{1,0:T(8,128)S(1)} %get-tuple-element.127), channel_id=1, source_target_pairs={{0,1},{1,2},{2,3},{3,0},{4,5},{5,6},{6,7},{7,4},{8,9},{9,10},{10,1... | collective-permute-start | bytes 12296 | tf_op jit(solution)/shard_map/ppermute | solution.py:29
  145.2 7.6 %collective-permute-start.29 = (f32[8,128]{1,0:T(8,128)S(1)}, f32[8,128]{1,0:T(8,128)S(1)}, u32[]{:S(2)}, u32[]{:S(2)}) collective-permute-start(f32[8,128]{1,0:T(8,128)S(1)} %get-tuple-element.127), channel_id=1, source_target_pairs={{0,3},{1,0},{2,1},{3,2},{4,7},{5,4},{6,5},{7,6},{8,11},{9,8},{10,9... | collective-permute-start | bytes 12296 | tf_op jit(solution)/shard_map/ppermute | solution.py:29
  148.9 4.0 %collective-permute-start.30 = (f32[8,128]{1,0:T(8,128)S(1)}, f32[8,128]{1,0:T(8,128)S(1)}, u32[]{:S(2)}, u32[]{:S(2)}) collective-permute-start(f32[8,128]{1,0:T(8,128)S(1)} %get-tuple-element.127), channel_id=1, source_target_pairs={{0,2},{1,3},{2,0},{3,1},{4,6},{5,7},{6,4},{7,5},{8,10},{9,11},{10,... | collective-permute-start | bytes 12296 | tf_op jit(solution)/shard_map/ppermute | solution.py:29
  148.9 19.2 %all-to-all-start.2 = ((bf16[32,32,256]{2,1,0:T(8,128)(2,1)}), bf16[32,32,256]{2,1,0:T(8,128)(2,1)S(1)}, u32[]{:S(2)}, u32[]{:S(2)}) async-start(bf16[32,32,256]{2,1,0:T(8,128)(2,1)} %add_convert_fusion), calls=%async_computation.2 | async-start | bytes 1048576 | tf_op jit(solution)/shard_map/all_to_all | solution.py:469
  153.0 11.1 %collective-permute-start.31 = (bf16[30,256]{1,0:T(8,128)(2,1)S(1)}, bf16[30,256]{1,0:T(8,128)(2,1)S(1)}, u32[]{:S(2)}, u32[]{:S(2)}) collective-permute-start(bf16[30,256]{1,0:T(8,128)(2,1)S(1)} %slice.30), channel_id=1, source_target_pairs={{4,0},{8,4},{12,8},{16,12},{20,16},{24,20},{28,24},{32,28},{36,32}... | collective-permute-start | bytes 46088 | tf_op jit(solution)/shard_map/ppermute | solution.py:478
  (32 other events, 59.1 us)
